TPU v7x, 32 devices: a whole 2x2x4 slice. The times are simulated.
32 devices in a mesh: sp: 8 (over z, y), tp: 4 (over x, core).
Axes of the slice: x: 2, y: 2, z: 4, core: 2. Of those that a mesh axis runs over, the one named last changes fastest.
Arguments:
- residual: bfloat16 [4096, 2048], P(('sp', 'tp')), may hold values from -6 to 6
- query_major: bfloat16 [4096, 1024], P('sp', 'tp'), may hold values from -160 to 160
- keys_major: bfloat16 [4096, 1024], P('sp', 'tp'), may hold values from -6.5 to 6.5
- values_major: bfloat16 [4096, 1024], P('sp', 'tp'), may hold values from -6 to 6
- query_minor: bfloat16 [4096, 512], P('sp', 'tp'), may hold values from -160 to 160
- keys_minor: bfloat16 [4096, 512], P('sp', 'tp'), may hold values from -6.5 to 6.5
- values_minor: bfloat16 [4096, 512], P('sp', 'tp'), may hold values from -6 to 6
- lambda_major: float32 [8], P('tp'), may hold values from 0.3 to 0.8
- lambda_minor: float32 [8], P('tp'), may hold values from 0.3 to 0.8
- gain_major: float32 [128], replicated, may hold values from 0.1 to 1.9
- gain_minor: float32 [64], replicated, may hold values from 0.1 to 1.9
- output_major: bfloat16 [1024, 2048], P('tp'), may hold values from -0.15625 to 0.15625
- output_minor: bfloat16 [512, 2048], P('tp'), may hold values from -0.15625 to 0.15625
- mixer_gain: float32 [2048], replicated, may hold values from 0.1 to 1.9
- up_weight: bfloat16 [2048, 8192], P('sp', 'tp'), may hold values from -0.125 to 0.125
- down_weight: bfloat16 [8192, 2048], P('tp', 'sp'), may hold values from -0.0625 to 0.0625
Outputs:
- layer_out: bfloat16 [4096, 2048], P(('sp', 'tp'))
All inputs are finite; a program needn't handle non-finite values.
Results may differ from a plain program's by a relative error of at most 0.018.
Values may be sent and summed in bfloat16 or wider, within the bound.
A program may use at most 128 MiB of HBM per device.

v0:
```python
import functools

import jax
import jax.numpy as jnp
from jax import lax
from jax.experimental import pallas as pl
from jax.experimental.pallas import tpu as pltpu
from jax.sharding import PartitionSpec as P

DK_MAJOR = 64
DK_MINOR = 32
SEGMENT = 64
MAPS = 2

EPSILON = 1e-06
NEGATIVE = -1e30
LOG2_E = 1.4426950408889634
ANY = pl.BlockSpec(memory_space=pl.ANY)
VMEM = pl.BlockSpec(memory_space=pltpu.VMEM)
SMEM = pl.BlockSpec(memory_space=pltpu.SMEM)


def grid_sizes(sp_count):
    y_count = 1 << ((sp_count.bit_length() - 1) // 2)
    return sp_count // y_count, y_count


class Gather:
    def __init__(self, sp_count, places, send_sem, recv_sem):
        self.z_count, self.y_count = grid_sizes(sp_count)
        own = lax.axis_index("sp")
        self.own, self.z, self.y = own, own // self.y_count, lax.rem(own, self.y_count)
        self.places, self.send_sem, self.recv_sem = places, send_sem, recv_sem
        self.copies = []

    def z_peer(self, step):
        return lax.rem(self.z + step, self.z_count) * self.y_count + self.y

    def y_peer(self, step):
        return self.z * self.y_count + lax.rem(self.y + step, self.y_count)

    def send(self, array, source, src_ref, target):
        copy = pltpu.make_async_remote_copy(
            src_ref=src_ref,
            dst_ref=self.places[array](source),
            send_sem=self.send_sem.at[array, len([c for c in self.copies if c[0] == array])],
            recv_sem=self.recv_sem.at[array, source],
            device_id={"sp": target},
            device_id_type=pl.DeviceIdType.MESH,
        )
        copy.start()
        self.copies.append((array, copy))

    def wait_block(self, array, source):
        place = self.places[array](source)
        pltpu.make_async_remote_copy(
            src_ref=place,
            dst_ref=place,
            send_sem=self.send_sem.at[array, 0],
            recv_sem=self.recv_sem.at[array, source],
            device_id={"sp": self.y_peer(1)},
            device_id_type=pl.DeviceIdType.MESH,
        ).wait_recv()

    def send_z(self, array, src_ref):
        for step in range(1, self.z_count):
            self.send(array, self.own, src_ref, self.z_peer(step))

    def send_y(self, array, src_ref):
        for step in range(1, self.y_count):
            self.send(array, self.own, src_ref, self.y_peer(step))

    def pass_on(self, array, step):
        source = self.z_peer(self.z_count - step)
        self.wait_block(array, source)
        for y_step in range(1, self.y_count):
            self.send(array, source, self.places[array](source), self.y_peer(y_step))

    def wait_y(self, array):
        for y_step in range(1, self.y_count):
            for z_step in range(self.z_count):
                z_at = lax.rem(self.z + z_step, self.z_count)
                self.wait_block(array, z_at * self.y_count + lax.rem(self.y + y_step, self.y_count))

    def finish(self):
        for _, copy in self.copies:
            copy.wait_send()


def mixer_kernel(
    sp_count,
    groups,
    q_major,
    k_major,
    v_major,
    q_minor,
    kv_minor,
    lam_major,
    lam_minor,
    gain_major,
    gain_minor,
    up_ref,
    down_ref,
    out_major,
    out_minor,
    up_all,
    down_all,
    k_major_all,
    v_major_all,
    kv_minor_all,
    qm_major,
    qm_minor,
    acc_major,
    acc_minor,
    peaks,
    totals,
    send_sem,
    recv_sem,
    local_sem,
):
    rows = q_major.shape[0]
    up_rows = up_ref.shape[0]

    def rows_of(ref, count):
        return lambda source: ref.at[pl.ds(pl.multiple_of(source * count, count), count), :]

    places = [
        rows_of(k_major_all, rows),
        rows_of(v_major_all, rows),
        rows_of(kv_minor_all, rows),
        rows_of(up_all, up_rows),
        lambda source: down_all.at[source],
    ]
    own_refs = [k_major, v_major, kv_minor, up_ref, down_ref]
    gather = Gather(sp_count, places, send_sem, recv_sem)
    own = gather.own

    barrier = pltpu.get_barrier_semaphore()
    peers = [gather.z_peer(step) for step in range(1, gather.z_count)]
    peers += [gather.y_peer(step) for step in range(1, gather.y_count)]
    for peer in peers:
        pl.semaphore_signal(
            barrier, inc=1, device_id={"sp": peer}, device_id_type=pl.DeviceIdType.MESH
        )
    pl.semaphore_wait(barrier, len(peers))

    for array in range(3):
        gather.send_z(array, own_refs[array])
    for array in range(3):
        gather.send_y(array, own_refs[array])
    for array in (3, 4):
        gather.send_z(array, own_refs[array])
    for array in (3, 4):
        gather.send_y(array, own_refs[array])
    local = []
    for slot, array in enumerate((3, 4)):
        copy = pltpu.make_async_copy(own_refs[array], places[array](own), local_sem.at[slot])
        copy.start()
        local.append(copy)

    heads = []
    for group, (head_count, key_size) in enumerate(groups):
        q_ref, qm_ref = ((q_major, qm_major), (q_minor, qm_minor))[group]
        acc_ref = (acc_major, acc_minor)[group]
        value_size = acc_ref.shape[1]
        lanes = qm_ref.shape[2]
        for head in range(head_count):
            first = head * MAPS * key_size
            lane_first = first // lanes * lanes
            block = q_ref[:, lane_first : lane_first + lanes]
            lane = lax.broadcasted_iota(jnp.int32, block.shape, 1) + lane_first
            for m in range(MAPS):
                low = first + m * key_size
                keep = (lane >= low) & (lane < low + key_size)
                picked = jnp.where(keep, block.astype(jnp.float32), 0.0).astype(block.dtype)
                qm_ref[head, m * rows : (m + 1) * rows, :] = picked
            heads.append((group, head, len(heads), lane_first, lanes, value_size, key_size))

    minor_keys = q_minor.shape[1]
    minor_first = minor_keys // 128 * 128

    def fold(key_refs, value_refs, at, diagonal):
        window = pl.ds(at, rows)
        stored = (value_refs[0][window, :], value_refs[1][window, minor_first:])
        turned = [jnp.transpose(v.astype(jnp.float32)).astype(jnp.bfloat16) for v in stored]
        turned[1] = turned[1][minor_keys - minor_first :, :]
        for group, head, index, lane_first, lanes, value_size, key_size in heads:
            qm_ref = (qm_major, qm_minor)[group]
            acc_ref = (acc_major, acc_minor)[group]
            keys = key_refs[group][window, lane_first : lane_first + lanes]
            values = turned[group][head * value_size : (head + 1) * value_size, :]
            scores = lax.dot_general(
                keys, qm_ref[head], (((1,), (1,)), ((), ())), preferred_element_type=jnp.float32
            ) * (key_size ** (-0.5) * LOG2_E)
            if diagonal:
                key_pos = lax.broadcasted_iota(jnp.int32, scores.shape, 0)
                query_pos = lax.broadcasted_iota(jnp.int32, scores.shape, 1) % rows
                visible = key_pos // SEGMENT <= query_pos // SEGMENT
                scores = jnp.where(visible, scores, NEGATIVE)
            peak = jnp.max(scores, axis=0, keepdims=True)
            if not diagonal:
                peak_old = peaks[index]
                peak = jnp.maximum(peak, peak_old)
            weights = jnp.exp2(scores - peak)
            total = jnp.sum(weights, axis=0, keepdims=True)
            sums = jnp.dot(
                values, weights.astype(jnp.bfloat16), preferred_element_type=jnp.float32
            )
            if not diagonal:
                factor = jnp.exp2(peak_old - peak)
                total = total + totals[index] * factor
                sums = sums + acc_ref[head] * factor
            peaks[index] = peak
            totals[index] = total
            acc_ref[head] = sums

    fold((k_major, kv_minor), (v_major, kv_minor), 0, True)

    for step in range(1, gather.z_count):
        for array in range(3):
            gather.pass_on(array, step)

    def earlier(block, carry):
        at = pl.multiple_of(block * rows, rows)
        fold((k_major_all, kv_minor_all), (v_major_all, kv_minor_all), at, False)
        return carry

    y_count = gather.y_count

    def same_y(z_at, carry):
        return earlier(z_at * y_count + gather.y, carry)

    def other_y(index, carry):
        z_at, place = index // (y_count - 1), lax.rem(index, y_count - 1)
        y_at = place + (place >= gather.y).astype(jnp.int32)
        return earlier(z_at * y_count + y_at, carry)

    lax.fori_loop(0, gather.z, same_y, 0)
    for array in range(3):
        gather.wait_y(array)
    lax.fori_loop(0, gather.z * (y_count - 1) + gather.y, other_y, 0)

    for group, (head_count, _) in enumerate(groups):
        acc_ref = (acc_major, acc_minor)[group]
        lam_ref = (lam_major, lam_minor)[group]
        gain_ref = (gain_major, gain_minor)[group]
        out_ref = (out_major, out_minor)[group]
        done = []
        for head in range(head_count):
            index = next(h[2] for h in heads if h[0] == group and h[1] == head)
            ratio = acc_ref[head] / totals[index]
            diff = ratio[:, :rows] - lam_ref[head] * ratio[:, rows:]
            mean = jnp.mean(diff * diff, axis=0, keepdims=True)
            done.append(diff * lax.rsqrt(mean + EPSILON) * gain_ref[...])
        out_ref[...] = jnp.transpose(jnp.concatenate(done, axis=0)).astype(out_ref.dtype)

    for step in range(1, gather.z_count):
        for array in (3, 4):
            gather.pass_on(array, step)
    for array in (3, 4):
        gather.wait_y(array)
    for copy in local:
        copy.wait()
    gather.finish()


def mixer(sp_count, *args):
    q_major, k_major, v_major, q_minor, kv_minor = args[:5]
    up_weight, down_weight = args[9:11]
    heads_major = k_major.shape[1] // (MAPS * DK_MAJOR)
    heads_minor = q_minor.shape[1] // (MAPS * DK_MINOR)
    rows = q_major.shape[0]
    size_major = v_major.shape[1] // heads_major
    width_minor = kv_minor.shape[1] - q_minor.shape[1]
    size_minor = width_minor // heads_minor
    lanes_major = min(MAPS * DK_MAJOR, q_major.shape[1])
    lanes_minor = min(128, q_minor.shape[1])
    z_count, y_count = grid_sizes(sp_count)
    sends = (z_count - 1) + (y_count - 1) * z_count
    tokens = rows * sp_count
    bf16, f32 = jnp.bfloat16, jnp.float32
    head_total = heads_major + heads_minor
    return pl.pallas_call(
        functools.partial(
            mixer_kernel, sp_count, ((heads_major, DK_MAJOR), (heads_minor, DK_MINOR))
        ),
        out_shape=(
            jax.ShapeDtypeStruct(v_major.shape, bf16),
            jax.ShapeDtypeStruct((rows, width_minor), bf16),
            jax.ShapeDtypeStruct((up_weight.shape[0] * sp_count, up_weight.shape[1]), bf16),
            jax.ShapeDtypeStruct((sp_count, *down_weight.shape), bf16),
        ),
        in_specs=[VMEM] * 5 + [SMEM] * 2 + [VMEM] * 4,
        out_specs=(VMEM, VMEM, ANY, ANY),
        scratch_shapes=[
            pltpu.VMEM((tokens, k_major.shape[1]), bf16),
            pltpu.VMEM((tokens, v_major.shape[1]), bf16),
            pltpu.VMEM((tokens, kv_minor.shape[1]), bf16),
            pltpu.VMEM((heads_major, MAPS * rows, lanes_major), bf16),
            pltpu.VMEM((heads_minor, MAPS * rows, lanes_minor), bf16),
            pltpu.VMEM((heads_major, size_major, MAPS * rows), f32),
            pltpu.VMEM((heads_minor, size_minor, MAPS * rows), f32),
            pltpu.VMEM((head_total, 1, MAPS * rows), f32),
            pltpu.VMEM((head_total, 1, MAPS * rows), f32),
            pltpu.SemaphoreType.DMA((5, sends)),
            pltpu.SemaphoreType.DMA((5, sp_count)),
            pltpu.SemaphoreType.DMA((2,)),
        ],
        compiler_params=pltpu.CompilerParams(
            collective_id=0, has_side_effects=True, vmem_limit_bytes=60 * 1024 * 1024
        ),
    )(*args)


class Exchange:
    def __init__(self, tp_count, send_sem, recv_sem):
        own = lax.axis_index("tp")
        self.x_count = tp_count // 2
        self.own, self.x, self.core = own, own // 2, lax.rem(own, 2)
        self.partner = self.x * 2 + 1 - self.core
        self.send_sem, self.recv_sem = send_sem, recv_sem

    def enter(self):
        barrier = pltpu.get_barrier_semaphore()
        peers = [self.partner] + [self.x_peer(step) for step in range(1, self.x_count)]
        for peer in peers:
            pl.semaphore_signal(
                barrier, inc=1, device_id={"tp": peer}, device_id_type=pl.DeviceIdType.MESH
            )
        pl.semaphore_wait(barrier, len(peers))

    def x_peer(self, step):
        return lax.rem(self.x + step, self.x_count) * 2 + self.core

    def copy(self, src, dst, slot, target):
        made = pltpu.make_async_remote_copy(
            src_ref=src,
            dst_ref=dst,
            send_sem=self.send_sem.at[slot],
            recv_sem=self.recv_sem.at[slot],
            device_id={"tp": target},
            device_id_type=pl.DeviceIdType.MESH,
        )
        made.start()
        return made

    def total(self, partial, pair_in, pair_sum, x_in, rows):
        def block(x_at, core):
            return pl.ds(pl.multiple_of((x_at * 2 + core) * rows, rows), rows)

        steps = list(range(1, self.x_count)) + [0]
        at = [lax.rem(self.x + step, self.x_count) for step in range(self.x_count)]
        pair = {}
        for step in steps:
            pair[step] = self.copy(
                partial.at[block(at[step], 1 - self.core), :], pair_in.at[step], step, self.partner
            )
        across = []
        for step in steps:
            pair[step].wait_recv()
            mine = partial[block(at[step], self.core), :].astype(jnp.float32)
            both = mine + pair_in[step].astype(jnp.float32)
            if step:
                pair_sum[step] = both.astype(jnp.bfloat16)
                across.append(
                    self.copy(
                        pair_sum.at[step], x_in.at[step], self.x_count + step, self.x_peer(step)
                    )
                )
        for made in across:
            made.wait_recv()
        for step in range(1, self.x_count):
            both = both + x_in[step].astype(jnp.float32)
        return both, list(pair.values()) + across


def mix_kernel(
    tp_count, partial, residual, gain, stream_ref, normed_ref, pair_in, pair_sum, x_in, held, send_sem, recv_sem
):
    exchange = Exchange(tp_count, send_sem, recv_sem)
    exchange.enter()
    rows = residual.shape[0]
    mixed, copies = exchange.total(partial, pair_in, pair_sum, x_in, rows)
    stream = residual[...].astype(jnp.float32) + mixed
    stream_ref[...] = stream
    mean = jnp.mean(stream * stream, axis=-1, keepdims=True)
    normed = (stream * lax.rsqrt(mean + EPSILON) * gain[...]).astype(jnp.bfloat16)
    held[...] = normed

    def place(index):
        return normed_ref.at[pl.ds(pl.multiple_of(index * rows, rows), rows), :]

    base, count = 2 * exchange.x_count, exchange.x_count
    sent = [exchange.copy(held, place(exchange.own), base + step, exchange.x_peer(step)) for step in range(1, count)]
    passed = [exchange.copy(held, place(exchange.own), base + count, exchange.partner)]
    normed_ref[pl.ds(pl.multiple_of(exchange.own * rows, rows), rows), :] = normed
    for step in range(1, count):
        sent[step - 1].wait_recv()
        source = exchange.x_peer(count - step)
        passed.append(
            exchange.copy(place(source), place(source), base + count + step, exchange.partner)
        )
    for made in passed:
        made.wait_recv()
    for made in copies + sent + passed:
        made.wait_send()


def sum_kernel(tp_count, partial, stream, out_ref, pair_in, pair_sum, x_in, send_sem, recv_sem):
    exchange = Exchange(tp_count, send_sem, recv_sem)
    exchange.enter()
    total, copies = exchange.total(partial, pair_in, pair_sum, x_in, stream.shape[0])
    out_ref[...] = (stream[...] + total).astype(out_ref.dtype)
    for made in copies:
        made.wait_send()


def tp_call(kernel, identity, inputs, out_shape, rows, holds):
    tp_count = lax.axis_size("tp")
    slots = (tp_count // 2, rows, inputs[0].shape[1])
    held = [pltpu.VMEM(slots[1:], jnp.bfloat16)] if holds else []
    return pl.pallas_call(
        functools.partial(kernel, tp_count),
        out_shape=out_shape,
        in_specs=[VMEM] * len(inputs),
        out_specs=jax.tree.map(lambda _: VMEM, out_shape),
        scratch_shapes=[pltpu.VMEM(slots, jnp.bfloat16)] * 3
        + held
        + [pltpu.SemaphoreType.DMA((2 * tp_count,))] * 2,
        compiler_params=pltpu.CompilerParams(
            collective_id=identity, has_side_effects=True, vmem_limit_bytes=32 * 1024 * 1024
        ),
    )(*inputs)


def body(
    residual,
    query_major,
    keys_major,
    values_major,
    query_minor,
    keys_minor,
    values_minor,
    lambda_major,
    lambda_minor,
    gain_major,
    gain_minor,
    output_major,
    output_minor,
    mixer_gain,
    up_weight,
    down_weight,
):
    out_major, out_minor, up_full, down_full = mixer(
        lax.axis_size("sp"),
        query_major,
        keys_major,
        values_major,
        query_minor,
        jnp.concatenate([keys_minor, values_minor], axis=1),
        lambda_major,
        lambda_minor,
        gain_major[:, None],
        gain_minor[:, None],
        up_weight,
        down_weight,
    )
    partial_sum = jnp.dot(out_major, output_major, preferred_element_type=jnp.float32)
    partial_sum = partial_sum + jnp.dot(out_minor, output_minor, preferred_element_type=jnp.float32)
    rows = residual.shape[0]
    stream, normed_all = tp_call(
        mix_kernel,
        1,
        (partial_sum.astype(jnp.bfloat16), residual, mixer_gain[None, :]),
        (
            jax.ShapeDtypeStruct(residual.shape, jnp.float32),
            jax.ShapeDtypeStruct(partial_sum.shape, jnp.bfloat16),
        ),
        rows,
        True,
    )
    pre_act = jnp.dot(
        normed_all,
        up_full,
        preferred_element_type=jnp.float32,
    )
    hidden = jnp.square(jax.nn.relu(pre_act)).astype(jnp.bfloat16)
    down_part = jnp.einsum("th,shd->tsd", hidden, down_full, preferred_element_type=jnp.float32)
    down_part = down_part.astype(jnp.bfloat16).reshape(partial_sum.shape)
    return tp_call(
        sum_kernel,
        2,
        (down_part, stream),
        jax.ShapeDtypeStruct(residual.shape, residual.dtype),
        rows,
        False,
    )


def solution(mesh):
    return jax.shard_map(
        body,
        mesh=mesh,
        in_specs=(
            P(("sp", "tp"), None),
            P("sp", "tp"),
            P("sp", "tp"),
            P("sp", "tp"),
            P("sp", "tp"),
            P("sp", "tp"),
            P("sp", "tp"),
            P("tp"),
            P("tp"),
            P(),
            P(),
            P("tp", None),
            P("tp", None),
            P(),
            P("sp", "tp"),
            P("tp", "sp"),
        ),
        out_specs=P(("sp", "tp"), None),
        check_vma=False,
    )
```

profile of v0, /device:TPU:16, one launch (start us, length us, event | category | flops | bytes accessed | tf_op | source)
XLA Modules:
  0.0 422.4 jit_solution(10502306863031613991)
XLA Ops:
  0.0 0.0 copy-start
  0.0 1.4 copy.18.gain_minor
  1.4 1.4 copy.17.gain_major
  2.8 1.7 pad_maximum_fusion.kv_minor
  4.5 345.9 %shard_map.154 = (bf16[512,256]{1,0:T(8,128)(2,1)}, bf16[512,128]{1,0:T(8,128)(2,1)}, bf16[2048,2048]{1,0:T(8,128)(2,1)}, bf16[8,2048,256]{2,1,0:T(8,128)(2,1)}) custom-call(bf16[512,256]{1,0:T(8,128)(2,1)} %q_major.1, bf16[512,256]{1,0:T(8,128)(2,1)} %k_major.1, bf16[512,256]{1,0:T(8,128)(2,1)} %v_major.1, bf16[512,128]{1,0:T(8,128)(2,1)} %q_minor.1, ...), custom_call_target="tpu_custom_call" | custom-call | tf_op jit(solution)/shard_map/pallas_call | solution.py:283
  350.5 0.0 copy-start.5
  350.5 0.0 copy-start.6
  350.5 0.0 copy-done
  350.5 1.7 fusion.2
  352.2 0.0 copy-done.5
  352.3 0.0 copy-done.6
  352.3 0.0 copy-start.3
  352.3 0.0 copy-start.4
  352.3 0.7 add_convert_fusion.partial
  353.0 0.3 copy-done.3
  353.3 0.0 copy-done.4
  353.3 30.8 %shard_map.155 = (f32[128,2048]{1,0:T(8,128)S(1)}, bf16[512,2048]{1,0:T(8,128)(2,1)S(1)}) custom-call(bf16[512,2048]{1,0:T(8,128)(2,1)S(1)} %add_convert_fusion.partial, bf16[128,2048]{1,0:T(8,128)(2,1)S(1)} %copy-done.3, f32[1,2048]{1,0:T(1,128)S(1)} %bitcast.15), custom_call_target="tpu_custom_call" | custom-call | tf_op jit(solution)/shard_map/pallas_call | solution.py:422
  384.1 0.0 copy-start.1
  384.1 1.0 copy-done.1
  385.1 16.0 %convolution_convert_fusion = bf16[512,8,256]{0,2,1:T(8,128)(2,1)} fusion(bf16[8,2048,256]{2,1,0:T(8,128)(2,1)} %get-tuple-element.15, bf16[512,2048]{1,0:T(8,128)(2,1)S(1)} %get-tuple-element.13, bf16[2048,2048]{1,0:T(8,128)(2,1)} %get-tuple-element.14), kind=kOutput, calls=%fused_computation.3 | convolution fusion | flops 8594128896 | bytes 20971520 | tf_op jit(solution)/shard_map/th,shd->tsd/dot_general | solution.py:488
  401.1 2.9 copy.22.partial
  404.0 1.2 copy-done.2
  405.2 16.4 %shard_map.156 = bf16[128,2048]{1,0:T(8,128)(2,1)S(1)} custom-call(bf16[512,2048]{1,0:T(8,128)(2,1)S(1)} %copy.22.partial, f32[128,2048]{1,0:T(8,128)S(1)} %copy-done.2), custom_call_target="tpu_custom_call" | custom-call | tf_op jit(solution)/shard_map/pallas_call | solution.py:422
  421.6 0.8 copy.24
  (1 shorter events, 0.0 us)
Async XLA Ops:
  0.0 350.5 %copy-start = (bf16[256,2048]{1,0:T(8,128)(2,1)S(1)}, bf16[256,2048]{1,0:T(8,128)(2,1)}, u32[]{:S(2)}) copy-start(bf16[256,2048]{1,0:T(8,128)(2,1)} %param.27) | copy-start | bytes 3145732
  350.5 1.8 copy-start.5
  350.5 1.8 copy-start.6
  352.3 1.0 copy-start.3
  352.3 1.0 copy-start.4
  384.1 1.0 copy-start.1
  404.0 1.2 copy-start.2
where the time goes:
time: 423 us; the launch traced here: 422 us
  Pallas kernels  393 us (93%)
  matrix products  18.4 us (4%)
  local copies, waits for them, and re-layouts  9.1 us (2%)
    pallas_call x1, Pallas kernels, mixer(): pl.pallas_call(functools.partial(mixer_kernel, sp_count, ((heads_major, D...  346 us
    pallas_call x2, Pallas kernels, tp_call(): pl.pallas_call(functools.partial(kernel, tp_count), out_shape=out_shape,...  47.2 us
    dot_general x1, matrix products, body(): jnp.einsum('th,shd->tsd', hidden, down_full, preferred_element_type=jnp.f...  16 us

commit v1 on v0

--- a/solution.py
+++ b/solution.py
@@ -433,6 +433,569 @@
     )(*inputs)
 
 
+class Sender:
+    def __init__(self, sem):
+        self.sem, self.made = sem, []
+
+    def prepare(self, src, dst, recv, target, when=None):
+        copy = pltpu.make_async_remote_copy(
+            src_ref=src,
+            dst_ref=dst,
+            send_sem=self.sem.at[len(self.made)],
+            recv_sem=recv,
+            device_id=target,
+            device_id_type=pl.DeviceIdType.MESH,
+        )
+        self.made.append((when, copy))
+        return lambda: run_when(when, copy.start)
+
+    def send(self, src, dst, recv, target, when=None):
+        self.prepare(src, dst, recv, target, when)()
+
+    def finish(self):
+        for when, copy in self.made:
+            run_when(when, copy.wait_send)
+
+
+def run_when(when, action):
+    if when is None:
+        action()
+    else:
+        pl.when(when)(lambda: action())
+
+
+def layer_kernel(
+    sizes,
+    residual,
+    q_major,
+    k_major,
+    v_major,
+    q_minor,
+    k_minor,
+    v_minor,
+    lam_major,
+    lam_minor,
+    gain_major,
+    gain_minor,
+    wo_major,
+    wo_minor,
+    mixer_gain,
+    up_ref,
+    down_ref,
+    out_ref,
+    pack,
+    kv_all,
+    q_in,
+    qm,
+    acc,
+    peaks,
+    totals,
+    heads_out,
+    cat,
+    minor_in,
+    wo_all,
+    stream,
+    normed_all,
+    up_all,
+    down_all,
+    hidden,
+    d_send,
+    d_in,
+    mine,
+    x_send,
+    x_in,
+    x_keep,
+    z_send,
+    z_in,
+    z_keep,
+    send_sem,
+    relay_sem,
+    local_sem,
+    r_y,
+    r_near,
+    r_far,
+    r_w,
+    r_wo,
+    r_h,
+    r_g,
+    r_d,
+    r_x,
+    r_z,
+):
+    z_count, y_count, x_count = sizes
+    bf16, f32 = jnp.bfloat16, jnp.float32
+    own, tp = lax.axis_index("sp"), lax.axis_index("tp")
+    z, y = own // y_count, lax.rem(own, y_count)
+    x, c = tp // 2, lax.rem(tp, 2)
+    oy, ox, oc = 1 - y, 1 - x, 1 - c
+    zl = lax.rem(z, 2)
+    oz = z + 1 - 2 * zl
+    rows, tile = q_major.shape[0], residual.shape[0]
+    width = q_minor.shape[1]
+    half = width // 2
+    hid = up_ref.shape[1] // 2
+    up_rows = up_ref.shape[0]
+    cols = down_ref.shape[1]
+
+    def dev(z_at=z, y_at=y, x_at=x, c_at=c):
+        return {"sp": z_at * y_count + y_at, "tp": x_at * 2 + c_at}
+
+    def span(start, count):
+        return pl.ds(pl.multiple_of(start * count, count), count)
+
+    def arrive(place, recv):
+        pltpu.make_async_remote_copy(
+            src_ref=place,
+            dst_ref=place,
+            send_sem=send_sem.at[0],
+            recv_sem=recv,
+            device_id=dev(y_at=oy),
+            device_id_type=pl.DeviceIdType.MESH,
+        ).wait_recv()
+
+    k_low = lax.broadcasted_iota(jnp.int32, (rows, width), 1)
+    for head in range(2):
+        k_part = (k_low >= head * half) & (k_low < (head + 1) * half)
+        turned_v = pltpu.roll(v_minor[...].astype(f32), half, 1)
+        pack[head] = jnp.where(k_part, k_minor[...].astype(f32), turned_v).astype(bf16)
+
+    barrier = pltpu.get_barrier_semaphore()
+    peers = []
+    for dy in range(2):
+        for dx in range(2):
+            for dc in range(2):
+                if dy or dx or dc:
+                    peers.append(dev(y_at=oy if dy else y, x_at=ox if dx else x, c_at=oc if dc else c))
+    peers += [dev(z_at=lax.rem(z + step, z_count)) for step in range(1, z_count)]
+    for peer in peers:
+        pl.semaphore_signal(barrier, inc=1, device_id=peer, device_id_type=pl.DeviceIdType.MESH)
+
+    kv_all[z, 0, span(y, rows), :] = k_major[:, span(y, width)]
+    kv_all[z, 1, span(y, rows), :] = v_major[:, span(y, width)]
+    kv_all[z, 2, span(y, rows), :] = pack[y]
+    local = []
+    local_pairs = [
+        (up_ref.at[:, span(zl, hid)], up_all.at[span(own, up_rows), :]),
+        (down_ref.at[span(zl, hid), :], down_all.at[own]),
+    ]
+    major_rows, minor_rows = wo_major.shape[0], wo_minor.shape[0]
+    tp_count = 2 * x_count
+    minor_base = tp_count * major_rows
+
+    def wo_place(part, index):
+        if part == 0:
+            return wo_all.at[span(index, major_rows), :]
+        return wo_all.at[pl.ds(pl.multiple_of(minor_base + index * minor_rows, minor_rows), minor_rows), :]
+
+    for part, ref in enumerate((wo_major, wo_minor)):
+        local_pairs.append((ref, wo_place(part, tp)))
+    for slot, (src, dst) in enumerate(local_pairs):
+        made = pltpu.make_async_copy(src, dst, local_sem.at[slot])
+        made.start()
+        local.append(made)
+
+    pl.semaphore_wait(barrier, len(peers))
+
+    sender = Sender(send_sem)
+    has_up = z < z_count - 1
+    next_z = jnp.minimum(z + 1, z_count - 1)
+
+    def kv_place(z_at, part, side):
+        return kv_all.at[z_at, part, span(side, rows), :]
+
+    for part, src in enumerate((k_major.at[:, span(oy, width)], v_major.at[:, span(oy, width)], pack.at[oy])):
+        sender.send(src, kv_place(z, part, y), r_y.at[part], dev(y_at=oy))
+    sender.send(q_major.at[:, span(oy, width)], q_in.at[0], r_y.at[3], dev(y_at=oy))
+    sender.send(q_minor, q_in.at[1], r_y.at[4], dev(y_at=oy))
+    for part, src in enumerate((k_major.at[:, span(y, width)], v_major.at[:, span(y, width)], pack.at[y])):
+        sender.send(src, kv_place(z, part, y), r_near.at[y, part], dev(z_at=next_z), has_up)
+
+    def weight_src(kind, z_at):
+        parity = span(lax.rem(z_at, 2), hid)
+        return up_ref.at[:, parity] if kind == 0 else down_ref.at[parity, :]
+
+    def weight_place(kind, source):
+        return up_all.at[span(source, up_rows), :] if kind == 0 else down_all.at[source]
+
+    def send_weight(kind, z_at, y_at, when=None):
+        return sender.prepare(
+            weight_src(kind, z_at), weight_place(kind, own), r_w.at[kind, own], dev(z_at=z_at, y_at=y_at), when
+        )
+
+    for kind in range(2):
+        for step in range(z_count - 1, 0, -1):
+            send_weight(kind, jnp.maximum(z - step, 0), y, z >= step)()
+    send_weight(0, z, oy)()
+    send_weight(1, z, oy)()
+    for part, ref in enumerate((wo_major, wo_minor)):
+        for dx, dc in ((0, 1), (1, 0), (1, 1)):
+            target = dev(x_at=ox if dx else x, c_at=oc if dc else c)
+            sender.send(ref, wo_place(part, tp), r_wo.at[part, tp], target)
+
+    up_sends = []
+    for kind in range(2):
+        for step in range(1 + kind, z_count):
+            z_at = jnp.minimum(z + step, z_count - 1)
+            up_sends.append(send_weight(kind, z_at, y, z + step < z_count))
+    late_send = send_weight(1, next_z, y, has_up)
+
+    scales = (DK_MAJOR ** (-0.5) * LOG2_E, DK_MINOR ** (-0.5) * LOG2_E)
+    lane = lax.broadcasted_iota(jnp.int32, (rows, width), 1)
+
+    def pick(group, side, block):
+        first, size = (0, DK_MAJOR) if group == 0 else (y * half, DK_MINOR)
+        for m in range(MAPS):
+            low = first + m * size
+            keep = (lane >= low) & (lane < low + size)
+            qm[group, side, m * rows : (m + 1) * rows, :] = jnp.where(keep, block.astype(f32), 0.0).astype(bf16)
+
+    def fold(side, z_at, key_side, diagonal):
+        window = span(key_side, rows)
+        for group in range(2):
+            keys = kv_all[z_at, 2 * group, window, :]
+            stored = kv_all[z_at, 1 + group, window, :]
+            values = jnp.transpose(stored.astype(f32)).astype(bf16)
+            scores = lax.dot_general(
+                keys, qm[group, side], (((1,), (1,)), ((), ())), preferred_element_type=f32
+            ) * scales[group]
+            if diagonal:
+                key_pos = lax.broadcasted_iota(jnp.int32, scores.shape, 0)
+                query_pos = lax.broadcasted_iota(jnp.int32, scores.shape, 1) % rows
+                visible = key_pos // SEGMENT <= query_pos // SEGMENT
+                scores = jnp.where(visible, scores, NEGATIVE)
+            peak = jnp.max(scores, axis=0, keepdims=True)
+            if not diagonal:
+                peak_old = peaks[group, side]
+                peak = jnp.maximum(peak, peak_old)
+            weights = jnp.exp2(scores - peak)
+            total = jnp.sum(weights, axis=0, keepdims=True)
+            sums = jnp.dot(values, weights.astype(bf16), preferred_element_type=f32)
+            if not diagonal:
+                factor = jnp.exp2(peak_old - peak)
+                total = total + totals[group, side] * factor
+                sums = sums + acc[group, side] * factor
+            peaks[group, side] = peak
+            totals[group, side] = total
+            acc[group, side] = sums
+
+    pick(0, y, q_major[:, span(y, width)])
+    pick(1, y, q_minor[...])
+
+    for part in range(3):
+        arrive(kv_place(z, part, oy), r_y.at[part])
+        sender.send(kv_place(z, part, oy), kv_place(z, part, oy), r_near.at[oy, part], dev(z_at=next_z), has_up)
+    for part in range(2):
+        arrive(q_in.at[part], r_y.at[3 + part])
+        pick(part, oy, q_in[part])
+
+    def issue_up():
+        for start in up_sends:
+            start()
+
+    pl.when(z == 0)(issue_up)
+
+    def diagonal_fold(side, carry):
+        fold(side, z, side, True)
+        return carry
+
+    lax.fori_loop(0, 2, diagonal_fold, 0)
+
+    def relay_copy(z_at):
+        return pltpu.make_async_remote_copy(
+            src_ref=kv_all.at[z_at],
+            dst_ref=kv_all.at[z_at],
+            send_sem=relay_sem.at[z_at],
+            recv_sem=r_far.at[z_at],
+            device_id=dev(z_at=next_z),
+            device_id_type=pl.DeviceIdType.MESH,
+        )
+
+    def inner(index, z_at):
+        fold(lax.rem(index, 2), z_at, index // 2, False)
+        return z_at
+
+    def earlier(step, carry):
+        z_at = z - step
+
+        @pl.when(step == 1)
+        def _():
+            for side in range(2):
+                for part in range(3):
+                    arrive(kv_place(z_at, part, side), r_near.at[side, part])
+
+        @pl.when(step > 1)
+        def _():
+            arrive(kv_all.at[z_at], r_far.at[z_at])
+
+        pl.when(has_up)(lambda: relay_copy(z_at).start())
+        pl.when(step == z)(issue_up)
+        lax.fori_loop(0, 4, inner, z_at)
+        return carry
+
+    fold(1, z, 0, False)
+    lax.fori_loop(1, z + 1, earlier, 0)
+
+    value_row = lax.broadcasted_iota(jnp.int32, (width, rows), 0)
+    value_keep = (value_row >= oy * half) & (value_row < (oy + 1) * half)
+    gains = (gain_major[...], gain_minor[...])
+    lams = (lam_major[y], lam_minor[y])
+
+    def close(side, carry):
+        for group in range(2):
+            ratio = acc[group, side] / totals[group, side]
+            diff = ratio[:, :rows] - lams[group] * ratio[:, rows:]
+            if group == 1:
+                diff = jnp.where(value_keep, diff, 0.0)
+            count = width if group == 0 else half
+            mean = jnp.sum(diff * diff, axis=0, keepdims=True) * (1.0 / count)
+            done = jnp.transpose(diff * lax.rsqrt(mean + EPSILON)) * gains[group]
+            heads_out[group, span(side, rows), :] = done.astype(bf16)
+        return carry
+
+    lax.fori_loop(0, 2, close, 0)
+
+    place = tp * y_count + y
+
+    def token_span(y_at, x_at, c_at):
+        return span(y_at * (rows // tile) + x_at * 2 + c_at, tile)
+
+    def head_place(group, index):
+        return cat.at[:, span(index, width)] if group == 0 else minor_in.at[index]
+
+    for dy, dx, dc in ((1, 1, 1), (1, 1, 0), (1, 0, 1), (1, 0, 0), (0, 1, 1), (0, 1, 0), (0, 0, 1)):
+        y_at, x_at, c_at = oy if dy else y, ox if dx else x, oc if dc else c
+        for group in range(2):
+            sender.send(
+                heads_out.at[group, token_span(y_at, x_at, c_at), :],
+                head_place(group, place),
+                r_h.at[group, place],
+                dev(y_at=y_at, x_at=x_at, c_at=c_at),
+            )
+    cat[:, span(place, width)] = heads_out[0, token_span(y, x, c), :]
+    minor_in[place] = heads_out[1, token_span(y, x, c), :]
+
+    def pass_weight(kind, z_at, when):
+        source = z_at * y_count + y
+        run_when(when, lambda: arrive(weight_place(kind, source), r_w.at[kind, source]))
+        sender.send(weight_place(kind, source), weight_place(kind, source), r_w.at[kind, source], dev(y_at=oy), when)
+
+    for step in range(1, z_count):
+        pass_weight(0, lax.rem(z + step, z_count), z + step < z_count)
+
+    for made in local:
+        made.wait()
+    for dx, dc in ((0, 1), (1, 0), (1, 1)):
+        index = (ox if dx else x) * 2 + (oc if dc else c)
+        for part in range(2):
+            arrive(wo_place(part, index), r_wo.at[part, index])
+    for dy, dx, dc in ((0, 0, 1), (0, 1, 0), (0, 1, 1), (1, 0, 0), (1, 0, 1), (1, 1, 0), (1, 1, 1)):
+        index = ((ox if dx else x) * 2 + (oc if dc else c)) * y_count + (oy if dy else y)
+        for group in range(2):
+            arrive(head_place(group, index), r_h.at[group, index])
+    major_width = tp_count * y_count * width
+    for index in range(tp_count):
+        both = minor_in[index * y_count].astype(f32) + minor_in[index * y_count + 1].astype(f32)
+        cat[:, major_width + index * width : major_width + (index + 1) * width] = pltpu.roll(both, half, 1).astype(bf16)
+
+    model = residual.shape[1]
+    step_cols = 256
+
+    def project(index, carry):
+        window = span(index, step_cols)
+        mixed = jnp.dot(cat[...], wo_all[:, window], preferred_element_type=f32)
+        added = residual[:, window].astype(f32) + mixed
+        stream[:, window] = added
+        return carry + jnp.sum(added * added, axis=1, keepdims=True)
+
+    square = lax.fori_loop(0, model // step_cols, project, jnp.zeros((tile, 1), f32))
+    norm = lax.rsqrt(square * (1.0 / model) + EPSILON)
+
+    def slot(c_at, x_at, zl_at):
+        return c_at * (2 * x_count) + x_at * 2 + zl_at
+
+    def rows_at(index):
+        return normed_all.at[span(index, tile), :]
+
+    mine_at = slot(c, x, zl)
+    normed_all[span(mine_at, tile), :] = (stream[...] * norm * mixer_gain[...]).astype(bf16)
+
+    def share(index, target):
+        sender.send(rows_at(index), rows_at(index), r_g.at[index], target)
+
+    partner, x_peer, z_peer = dev(c_at=oc), dev(x_at=ox), dev(z_at=oz)
+    share(mine_at, z_peer)
+    share(mine_at, x_peer)
+    share(mine_at, partner)
+    late_send()
+    index = slot(c, ox, zl)
+    arrive(rows_at(index), r_g.at[index])
+    share(index, partner)
+    index = slot(c, x, 1 - zl)
+    arrive(rows_at(index), r_g.at[index])
+    share(index, x_peer)
+    share(index, partner)
+    for step in range(1, z_count):
+        pass_weight(0, lax.rem(z + step, z_count), z + step >= z_count)
+    index = slot(c, ox, 1 - zl)
+    arrive(rows_at(index), r_g.at[index])
+    share(index, partner)
+    for step in range(z_count):
+        source = lax.rem(z + step, z_count) * y_count + oy
+        arrive(weight_place(0, source), r_w.at[0, source])
+
+    group_rows = 2 * x_count * tile
+    hid_cols = 256
+
+    def expand(side):
+        def one(index, carry):
+            window = span(index, hid_cols)
+            pre = jnp.dot(
+                normed_all[span(side, group_rows), :], up_all[:, window], preferred_element_type=f32
+            )
+            hidden[span(side, group_rows), window] = jnp.square(jnp.maximum(pre, 0.0)).astype(bf16)
+            return carry
+
+        lax.fori_loop(0, hid // hid_cols, one, 0)
+
+    expand(c)
+    for x_at in range(x_count):
+        for zl_at in range(2):
+            index = slot(oc, x_at, zl_at)
+            arrive(rows_at(index), r_g.at[index])
+    expand(oc)
+
+    x_rows = 2 * tile
+    blocks = []
+
+    def stage_x(t):
+        arrive(d_in.at[t], r_d.at[t])
+        x_send[t] = (mine[t, span(ox, x_rows), :] + d_in[t, span(ox, x_rows), :].astype(f32)).astype(bf16)
+        sender.send(x_send.at[t], x_in.at[t], r_x.at[t], x_peer)
+        x_keep[t] = mine[t, span(x, x_rows), :] + d_in[t, span(x, x_rows), :].astype(f32)
+
+    def stage_z(t):
+        arrive(x_in.at[t], r_x.at[t])
+        other, same = span(1 - zl, tile), span(zl, tile)
+        z_send[t] = (x_keep[t, other, :] + x_in[t, other, :].astype(f32)).astype(bf16)
+        sender.send(z_send.at[t], z_in.at[blocks[t]], r_z.at[blocks[t]], z_peer)
+        z_keep[t] = x_keep[t, same, :] + x_in[t, same, :].astype(f32)
+
+    def stage_end(t):
+        arrive(z_in.at[blocks[t]], r_z.at[blocks[t]])
+        window = span(blocks[t], cols)
+        total = stream[:, window] + (z_keep[t] + z_in[blocks[t]].astype(f32))
+        out_ref[:, window] = total.astype(out_ref.dtype)
+
+    def advance(t):
+        for stage, lag in ((stage_x, 1), (stage_z, 2), (stage_end, 3)):
+            if 0 <= t - lag < z_count * y_count:
+                stage(t - lag)
+
+    for t in range(z_count * y_count):
+        z_at = lax.rem(z - zl + 1 + t // 2, z_count)
+        source = z_at * y_count + (oy if t % 2 else y)
+        blocks.append(source)
+        if t % 2:
+            arrive(down_all.at[source], r_w.at[1, source])
+        else:
+            pass_weight(1, z_at, z_at != z)
+        d_send[t] = jnp.dot(
+            hidden[span(oc, group_rows), :], down_all[source], preferred_element_type=f32
+        ).astype(bf16)
+        sender.send(d_send.at[t], d_in.at[t], r_d.at[t], partner)
+        mine[t] = jnp.dot(hidden[span(c, group_rows), :], down_all[source], preferred_element_type=f32)
+        advance(t)
+    for t in range(z_count * y_count, z_count * y_count + 3):
+        advance(t)
+
+    sender.finish()
+    for step in range(1, z_count):
+        source = jnp.maximum(z - step, 0)
+        run_when((z >= step) & has_up, relay_copy(source).wait_send)
+
+
+def fused(sp_count, tp_count, args):
+    residual, q_major, _, v_major, q_minor = args[:5]
+    wo_major, wo_minor, _, up_weight, down_weight = args[11:16]
+    z_count, y_count = grid_sizes(sp_count)
+    x_count = tp_count // 2
+    rows, tile, width = q_major.shape[0], residual.shape[0], q_minor.shape[1]
+    model, hid = residual.shape[1], up_weight.shape[1] // 2
+    cols = down_weight.shape[1]
+    features = tp_count * (wo_major.shape[0] + wo_minor.shape[0])
+    group_rows = 2 * x_count * tile
+    steps = sp_count
+    bf16, f32 = jnp.bfloat16, jnp.float32
+    dma = pltpu.SemaphoreType.DMA
+    sends = 128
+    hbm = pl.BlockSpec(memory_space=pltpu.HBM)
+    return pl.pallas_call(
+        functools.partial(layer_kernel, (z_count, y_count, x_count)),
+        out_shape=jax.ShapeDtypeStruct(residual.shape, residual.dtype),
+        in_specs=[VMEM] * 7 + [SMEM] * 2 + [VMEM] * 2 + [hbm] * 2 + [VMEM] + [hbm] * 2,
+        out_specs=VMEM,
+        scratch_shapes=[
+            pltpu.VMEM((2, rows, width), bf16),
+            pltpu.VMEM((z_count, 3, y_count * rows, width), bf16),
+            pltpu.VMEM((2, rows, width), bf16),
+            pltpu.VMEM((2, 2, MAPS * rows, width), bf16),
+            pltpu.VMEM((2, 2, width, MAPS * rows), f32),
+            pltpu.VMEM((2, 2, 1, MAPS * rows), f32),
+            pltpu.VMEM((2, 2, 1, MAPS * rows), f32),
+            pltpu.VMEM((2, y_count * rows, width), bf16),
+            pltpu.VMEM((tile, features), bf16),
+            pltpu.VMEM((tp_count * y_count, tile, width), bf16),
+            pltpu.VMEM((features, model), bf16),
+            pltpu.VMEM((tile, model), f32),
+            pltpu.VMEM((2 * group_rows, model), bf16),
+            pltpu.VMEM((model, hid), bf16),
+            pltpu.VMEM((sp_count, hid, cols), bf16),
+            pltpu.VMEM((2 * group_rows, hid), bf16),
+            pltpu.VMEM((steps, group_rows, cols), bf16),
+            pltpu.VMEM((steps, group_rows, cols), bf16),
+            pltpu.VMEM((steps, group_rows, cols), f32),
+            pltpu.VMEM((steps, 2 * tile, cols), bf16),
+            pltpu.VMEM((steps, 2 * tile, cols), bf16),
+            pltpu.VMEM((steps, 2 * tile, cols), f32),
+            pltpu.VMEM((steps, tile, cols), bf16),
+            pltpu.VMEM((steps, tile, cols), bf16),
+            pltpu.VMEM((steps, tile, cols), f32),
+            dma((sends,)),
+            dma((z_count,)),
+            dma((4,)),
+            dma((5,)),
+            dma((2, 3)),
+            dma((z_count,)),
+            dma((2, sp_count)),
+            dma((2, tp_count)),
+            dma((2, tp_count * y_count)),
+            dma((2 * group_rows // tile,)),
+            dma((steps,)),
+            dma((steps,)),
+            dma((steps,)),
+        ],
+        compiler_params=pltpu.CompilerParams(
+            collective_id=0, has_side_effects=True, vmem_limit_bytes=63 * 1024 * 1024
+        ),
+    )(*args)
+
+
+def fits_fused(sp_count, tp_count, args):
+    q_major, k_major, v_major, q_minor, k_minor, v_minor = args[1:7]
+    z_count, y_count = grid_sizes(sp_count)
+    width = q_minor.shape[1]
+    return (
+        y_count == 2
+        and tp_count == 4
+        and z_count % 2 == 0
+        and width == 2 * MAPS * DK_MINOR
+        and width == MAPS * DK_MAJOR
+        and width % 128 == 0
+        and v_minor.shape[1] == width
+        and q_major.shape[1] == v_major.shape[1] == 2 * width
+    )
+
+
 def body(
     residual,
     query_major,
@@ -451,6 +1014,27 @@
     up_weight,
     down_weight,
 ):
+    sp_count, tp_count = lax.axis_size("sp"), lax.axis_size("tp")
+    args = (
+        residual,
+        query_major,
+        keys_major,
+        values_major,
+        query_minor,
+        keys_minor,
+        values_minor,
+        lambda_major,
+        lambda_minor,
+        gain_major[None, :],
+        jnp.tile(gain_minor, 2)[None, :],
+        output_major,
+        output_minor,
+        mixer_gain[None, :],
+        up_weight,
+        down_weight,
+    )
+    if fits_fused(sp_count, tp_count, args):
+        return fused(sp_count, tp_count, args)
     out_major, out_minor, up_full, down_full = mixer(
         lax.axis_size("sp"),
         query_major,

time: 423 us -> 261 us (0.62)
  Pallas kernels: 393 us -> 258 us
  matrix products: 18.4 us -> 0 us
  local copies, waits for them, and re-layouts: 9.1 us -> 3.13 us
    pallas_call x3 -> x1, Pallas kernels: 393 us -> 258 us  [fused(): pl.pallas_call(functools.partial(layer_kernel, (z_count, y_count, x_count...]
    dot_general x3 -> x0, matrix products: 18.4 us -> none  [the longest x1 16 us: body(): jnp.einsum('th,shd->tsd', hidden, down_full, preferred_element_type=jnp.f...]
where the time goes in v1:
time: 261 us
  Pallas kernels  258 us (99%)
  local copies, waits for them, and re-layouts  3.13 us (1%)
    pallas_call x1, Pallas kernels, fused(): pl.pallas_call(functools.partial(layer_kernel, (z_count, y_count, x_count...  258 us

profile of v1, /device:TPU:16, one launch (start us, length us, event | category | flops | bytes accessed | tf_op | source)
XLA Modules:
  0.0 261.2 jit_solution(15442262848295063841)
XLA Ops:
  0.0 0.0 copy-start
  0.0 0.7 copy-done
  0.7 0.6 broadcast_in_dim_tile.3.gain_minor
  1.3 258.0 %shard_map.154 = bf16[128,2048]{1,0:T(8,128)(2,1)} custom-call(bf16[128,2048]{1,0:T(8,128)(2,1)} %residual.1, bf16[512,256]{1,0:T(8,128)(2,1)} %q_major.1, bf16[512,256]{1,0:T(8,128)(2,1)} %k_major.1, bf16[512,256]{1,0:T(8,128)(2,1)} %v_major.1, bf16[512,128]{1,0:T(8,128)(2,1)} %q_minor.1, bf16[512,128]{1,0:T(8,128)(2,1)} %k_minor.1, ...), custom_call_target="tpu_custom_call" | custom-call | tf_op jit(solution)/shard_map/pallas_call | solution.py:932
  259.3 1.9 copy.18
  (1 shorter events, 0.0 us)
Async XLA Ops:
  0.0 0.7 copy-start

commit v2 on v1

--- a/solution.py
+++ b/solution.py
@@ -11,6 +11,7 @@
 DK_MINOR = 32
 SEGMENT = 64
 MAPS = 2
+DOWN_PARTS = 2
 
 EPSILON = 1e-06
 NEGATIVE = -1e30
@@ -512,8 +513,7 @@
     relay_sem,
     local_sem,
     r_y,
-    r_near,
-    r_far,
+    r_kv,
     r_w,
     r_wo,
     r_h,
@@ -521,6 +521,7 @@
     r_d,
     r_x,
     r_z,
+    credits,
 ):
     z_count, y_count, x_count = sizes
     bf16, f32 = jnp.bfloat16, jnp.float32
@@ -608,36 +609,53 @@
     sender.send(q_major.at[:, span(oy, width)], q_in.at[0], r_y.at[3], dev(y_at=oy))
     sender.send(q_minor, q_in.at[1], r_y.at[4], dev(y_at=oy))
     for part, src in enumerate((k_major.at[:, span(y, width)], v_major.at[:, span(y, width)], pack.at[y])):
-        sender.send(src, kv_place(z, part, y), r_near.at[y, part], dev(z_at=next_z), has_up)
+        sender.send(src, kv_place(z, part, y), r_kv.at[z, y, part], dev(z_at=next_z), has_up)
+
+    part_rows = hid // DOWN_PARTS
 
     def weight_src(kind, z_at):
-        parity = span(lax.rem(z_at, 2), hid)
-        return up_ref.at[:, parity] if kind == 0 else down_ref.at[parity, :]
+        parity = lax.rem(z_at, 2)
+        if kind == 0:
+            return up_ref.at[:, span(parity, hid)]
+        return down_ref.at[span(parity * DOWN_PARTS + kind - 1, part_rows), :]
 
     def weight_place(kind, source):
-        return up_all.at[span(source, up_rows), :] if kind == 0 else down_all.at[source]
+        if kind == 0:
+            return up_all.at[span(source, up_rows), :]
+        return down_all.at[source, (kind - 1) * part_rows : kind * part_rows, :]
 
     def send_weight(kind, z_at, y_at, when=None):
         return sender.prepare(
             weight_src(kind, z_at), weight_place(kind, own), r_w.at[kind, own], dev(z_at=z_at, y_at=y_at), when
         )
 
-    for kind in range(2):
-        for step in range(z_count - 1, 0, -1):
-            send_weight(kind, jnp.maximum(z - step, 0), y, z >= step)()
-    send_weight(0, z, oy)()
-    send_weight(1, z, oy)()
+    down_kinds = tuple(range(1, 1 + DOWN_PARTS))
+
+    def below(kinds):
+        return [
+            send_weight(kind, jnp.maximum(z - step, 0), y, z >= step)
+            for kind in kinds
+            for step in range(z_count - 1, 0, -1)
+        ]
+
+    def above(kinds, step, odd=None):
+        when = z + step < z_count
+        if odd is not None:
+            when = when & (lax.rem(z + step, 2) == odd)
+        return [send_weight(kind, jnp.minimum(z + step, z_count - 1), y, when) for kind in kinds]
+
+    def issue(starts):
+        for start in starts:
+            start()
+
+    issue(below((0,)))
+    for kind in (0, *down_kinds):
+        send_weight(kind, z, oy)()
     for part, ref in enumerate((wo_major, wo_minor)):
-        for dx, dc in ((0, 1), (1, 0), (1, 1)):
-            target = dev(x_at=ox if dx else x, c_at=oc if dc else c)
-            sender.send(ref, wo_place(part, tp), r_wo.at[part, tp], target)
-
-    up_sends = []
-    for kind in range(2):
-        for step in range(1 + kind, z_count):
-            z_at = jnp.minimum(z + step, z_count - 1)
-            up_sends.append(send_weight(kind, z_at, y, z + step < z_count))
-    late_send = send_weight(1, next_z, y, has_up)
+        sender.send(ref, wo_place(part, tp), r_wo.at[part, tp], dev(x_at=ox))
+        sender.send(ref, wo_place(part, tp), r_wo.at[part, tp], dev(c_at=oc))
+    below_down = below(down_kinds)
+    near_up = above((0,), 1)
 
     scales = (DK_MAJOR ** (-0.5) * LOG2_E, DK_MINOR ** (-0.5) * LOG2_E)
     lane = lax.broadcasted_iota(jnp.int32, (rows, width), 1)
@@ -680,60 +698,72 @@
 
     pick(0, y, q_major[:, span(y, width)])
     pick(1, y, q_minor[...])
+    fold(y, z, y, True)
 
     for part in range(3):
         arrive(kv_place(z, part, oy), r_y.at[part])
-        sender.send(kv_place(z, part, oy), kv_place(z, part, oy), r_near.at[oy, part], dev(z_at=next_z), has_up)
+        sender.send(kv_place(z, part, oy), kv_place(z, part, oy), r_kv.at[z, oy, part], dev(z_at=next_z), has_up)
+
+    def credit(kind, back):
+        pl.semaphore_signal(
+            credits.at[kind, z],
+            inc=1,
+            device_id=dev(z_at=jnp.maximum(z - back, 0)),
+            device_id_type=pl.DeviceIdType.MESH,
+        )
+
+    def await_credit(kind, step):
+        pl.semaphore_wait(credits.at[kind, jnp.minimum(z + step, z_count - 1)], 1)
+
+    def relay_copy(z_at, side, part):
+        return pltpu.make_async_remote_copy(
+            src_ref=kv_place(z_at, part, side),
+            dst_ref=kv_place(z_at, part, side),
+            send_sem=relay_sem.at[z_at, side, part],
+            recv_sem=r_kv.at[z_at, side, part],
+            device_id=dev(z_at=next_z),
+            device_id_type=pl.DeviceIdType.MESH,
+        )
+
+    def take(z_at, side):
+        for part in range(3):
+            arrive(kv_place(z_at, part, side), r_kv.at[z_at, side, part])
+            run_when(has_up, relay_copy(z_at, side, part).start)
+
+    def after_last():
+        issue(near_up)
+        for back in range(2, z_count):
+            run_when(z >= back, lambda: credit(0, back))
+        issue(below_down)
+
     for part in range(2):
         arrive(q_in.at[part], r_y.at[3 + part])
         pick(part, oy, q_in[part])
 
-    def issue_up():
-        for start in up_sends:
-            start()
-
-    pl.when(z == 0)(issue_up)
-
-    def diagonal_fold(side, carry):
-        fold(side, z, side, True)
+    pl.when(z == 0)(lambda: issue(near_up))
+
+    @pl.when(z > 0)
+    def _():
+        for side in range(2):
+            take(z - 1, side)
+
+    pl.when(z == 1)(after_last)
+    fold(oy, z, oy, True)
+    fold(1, z, 0, False)
+
+    def earlier(index, carry):
+        z_at, key_side = z - 1 - index // 2, lax.rem(index, 2)
+        pl.when(index > 1)(lambda: take(z_at, key_side))
+        pl.when((index == 2 * z - 1) & (z > 1))(after_last)
+
+        def inner(side, carry):
+            fold(side, z_at, key_side, False)
+            return carry
+
+        lax.fori_loop(0, 2, inner, 0)
         return carry
 
-    lax.fori_loop(0, 2, diagonal_fold, 0)
-
-    def relay_copy(z_at):
-        return pltpu.make_async_remote_copy(
-            src_ref=kv_all.at[z_at],
-            dst_ref=kv_all.at[z_at],
-            send_sem=relay_sem.at[z_at],
-            recv_sem=r_far.at[z_at],
-            device_id=dev(z_at=next_z),
-            device_id_type=pl.DeviceIdType.MESH,
-        )
-
-    def inner(index, z_at):
-        fold(lax.rem(index, 2), z_at, index // 2, False)
-        return z_at
-
-    def earlier(step, carry):
-        z_at = z - step
-
-        @pl.when(step == 1)
-        def _():
-            for side in range(2):
-                for part in range(3):
-                    arrive(kv_place(z_at, part, side), r_near.at[side, part])
-
-        @pl.when(step > 1)
-        def _():
-            arrive(kv_all.at[z_at], r_far.at[z_at])
-
-        pl.when(has_up)(lambda: relay_copy(z_at).start())
-        pl.when(step == z)(issue_up)
-        lax.fori_loop(0, 4, inner, z_at)
-        return carry
-
-    fold(1, z, 0, False)
-    lax.fori_loop(1, z + 1, earlier, 0)
+    lax.fori_loop(0, 2 * z, earlier, 0)
 
     value_row = lax.broadcasted_iota(jnp.int32, (width, rows), 0)
     value_keep = (value_row >= oy * half) & (value_row < (oy + 1) * half)
@@ -781,11 +811,19 @@
 
     for step in range(1, z_count):
         pass_weight(0, lax.rem(z + step, z_count), z + step < z_count)
+    for step in range(2, z_count):
+        run_when(z + step < z_count, lambda: await_credit(0, step))
+        issue(above((0,), step))
+    for step in range(2, z_count):
+        issue(above(down_kinds, step, 0))
 
     for made in local:
         made.wait()
-    for dx, dc in ((0, 1), (1, 0), (1, 1)):
-        index = (ox if dx else x) * 2 + (oc if dc else c)
+    for part in range(2):
+        index = ox * 2 + c
+        arrive(wo_place(part, index), r_wo.at[part, index])
+        sender.send(wo_place(part, index), wo_place(part, index), r_wo.at[part, index], dev(c_at=oc))
+    for index in (x * 2 + oc, ox * 2 + oc):
         for part in range(2):
             arrive(wo_place(part, index), r_wo.at[part, index])
     for dy, dx, dc in ((0, 0, 1), (0, 1, 0), (0, 1, 1), (1, 0, 0), (1, 0, 1), (1, 1, 0), (1, 1, 1)):
@@ -826,7 +864,9 @@
     share(mine_at, z_peer)
     share(mine_at, x_peer)
     share(mine_at, partner)
-    late_send()
+    issue(above(down_kinds, 1))
+    for step in range(1, z_count):
+        pass_weight(0, lax.rem(z + step, z_count), z + step >= z_count)
     index = slot(c, ox, zl)
     arrive(rows_at(index), r_g.at[index])
     share(index, partner)
@@ -834,14 +874,18 @@
     arrive(rows_at(index), r_g.at[index])
     share(index, x_peer)
     share(index, partner)
-    for step in range(1, z_count):
-        pass_weight(0, lax.rem(z + step, z_count), z + step >= z_count)
+    for back in range(2, z_count):
+        run_when((z >= back) & (zl == 1), lambda: credit(1, back))
     index = slot(c, ox, 1 - zl)
     arrive(rows_at(index), r_g.at[index])
     share(index, partner)
     for step in range(z_count):
         source = lax.rem(z + step, z_count) * y_count + oy
         arrive(weight_place(0, source), r_w.at[0, source])
+
+    for step in range(2, z_count):
+        run_when((z + step < z_count) & (lax.rem(z + step, 2) == 1), lambda: await_credit(1, step))
+        issue(above(down_kinds, step, 1))
 
     group_rows = 2 * x_count * tile
     hid_cols = 256
@@ -891,14 +935,25 @@
             if 0 <= t - lag < z_count * y_count:
                 stage(t - lag)
 
+    def z_of(t):
+        return z - zl + 1 - t // 2 if t < 4 else lax.rem(z - zl + t // 2, z_count)
+
+    def pass_down(t):
+        for kind in down_kinds:
+            pass_weight(kind, z_of(t), z_of(t) != z if t < 4 else None)
+
+    early_pass = {0: (0, 2), 1: (4,)}
+    for t in range(2, z_count * y_count):
+        if 2 * t + 2 < z_count * y_count:
+            early_pass[t] = (2 * t + 2,)
     for t in range(z_count * y_count):
-        z_at = lax.rem(z - zl + 1 + t // 2, z_count)
-        source = z_at * y_count + (oy if t % 2 else y)
+        source = z_of(t) * y_count + (oy if t % 2 else y)
         blocks.append(source)
+        for ahead in early_pass.get(t, ()):
+            pass_down(ahead)
         if t % 2:
-            arrive(down_all.at[source], r_w.at[1, source])
-        else:
-            pass_weight(1, z_at, z_at != z)
+            for kind in down_kinds:
+                arrive(weight_place(kind, source), r_w.at[kind, source])
         d_send[t] = jnp.dot(
             hidden[span(oc, group_rows), :], down_all[source], preferred_element_type=f32
         ).astype(bf16)
@@ -910,8 +965,10 @@
 
     sender.finish()
     for step in range(1, z_count):
-        source = jnp.maximum(z - step, 0)
-        run_when((z >= step) & has_up, relay_copy(source).wait_send)
+        for side in range(2):
+            for part in range(3):
+                copy = relay_copy(jnp.maximum(z - step, 0), side, part)
+                run_when((z >= step) & has_up, copy.wait_send)
 
 
 def fused(sp_count, tp_count, args):
@@ -927,7 +984,7 @@
     steps = sp_count
     bf16, f32 = jnp.bfloat16, jnp.float32
     dma = pltpu.SemaphoreType.DMA
-    sends = 128
+    sends = 160
     hbm = pl.BlockSpec(memory_space=pltpu.HBM)
     return pl.pallas_call(
         functools.partial(layer_kernel, (z_count, y_count, x_count)),
@@ -961,18 +1018,18 @@
             pltpu.VMEM((steps, tile, cols), bf16),
             pltpu.VMEM((steps, tile, cols), f32),
             dma((sends,)),
-            dma((z_count,)),
+            dma((z_count, 2, 3)),
             dma((4,)),
             dma((5,)),
-            dma((2, 3)),
-            dma((z_count,)),
-            dma((2, sp_count)),
+            dma((z_count, 2, 3)),
+            dma((1 + DOWN_PARTS, sp_count)),
             dma((2, tp_count)),
             dma((2, tp_count * y_count)),
             dma((2 * group_rows // tile,)),
             dma((steps,)),
             dma((steps,)),
             dma((steps,)),
+            pltpu.SemaphoreType.REGULAR((2, z_count)),
         ],
         compiler_params=pltpu.CompilerParams(
             collective_id=0, has_side_effects=True, vmem_limit_bytes=63 * 1024 * 1024

time: 261 us -> 182 us (0.70)
  Pallas kernels: 258 us -> 179 us
    pallas_call x1, Pallas kernels: 258 us -> 179 us  [fused(): pl.pallas_call(functools.partial(layer_kernel, (z_count, y_count, x_count...]
where the time goes in v2:
time: 182 us
  Pallas kernels  179 us (98%)
  local copies, waits for them, and re-layouts  3.13 us (2%)
    pallas_call x1, Pallas kernels, fused(): pl.pallas_call(functools.partial(layer_kernel, (z_count, y_count, x_count...  179 us

profile of v2, /device:TPU:16, one launch (start us, length us, event | category | flops | bytes accessed | tf_op | source)
XLA Modules:
  0.0 182.0 jit_solution(3311240409170423266)
XLA Ops:
  0.0 0.0 copy-start
  0.0 0.7 copy-done
  0.7 0.6 broadcast_in_dim_tile.3.gain_minor
  1.3 178.9 %shard_map.154 = bf16[128,2048]{1,0:T(8,128)(2,1)} custom-call(bf16[128,2048]{1,0:T(8,128)(2,1)} %residual.1, bf16[512,256]{1,0:T(8,128)(2,1)} %q_major.1, bf16[512,256]{1,0:T(8,128)(2,1)} %k_major.1, bf16[512,256]{1,0:T(8,128)(2,1)} %v_major.1, bf16[512,128]{1,0:T(8,128)(2,1)} %q_minor.1, bf16[512,128]{1,0:T(8,128)(2,1)} %k_minor.1, ...), custom_call_target="tpu_custom_call" | custom-call | tf_op jit(solution)/shard_map/pallas_call | solution.py:989
  180.1 1.9 %copy.18 = bf16[128,2048]{1,0:T(8,128)(2,1)} copy(bf16[128,2048]{1,0:T(8,128)(2,1)} %shard_map.154) | data formatting | bytes 1048576
  (1 shorter events, 0.0 us)
Async XLA Ops:
  0.0 0.7 copy-start

commit v3 on v2

--- a/solution.py
+++ b/solution.py
@@ -11,7 +11,7 @@
 DK_MINOR = 32
 SEGMENT = 64
 MAPS = 2
-DOWN_PARTS = 2
+PARTS = 2
 
 EPSILON = 1e-06
 NEGATIVE = -1e30
@@ -611,31 +611,30 @@
     for part, src in enumerate((k_major.at[:, span(y, width)], v_major.at[:, span(y, width)], pack.at[y])):
         sender.send(src, kv_place(z, part, y), r_kv.at[z, y, part], dev(z_at=next_z), has_up)
 
-    part_rows = hid // DOWN_PARTS
+    up_part, down_part = up_rows // PARTS, hid // PARTS
+    up_kinds, down_kinds = tuple(range(PARTS)), tuple(range(PARTS, 2 * PARTS))
 
     def weight_src(kind, z_at):
         parity = lax.rem(z_at, 2)
-        if kind == 0:
-            return up_ref.at[:, span(parity, hid)]
-        return down_ref.at[span(parity * DOWN_PARTS + kind - 1, part_rows), :]
+        if kind < PARTS:
+            return up_ref.at[kind * up_part : (kind + 1) * up_part, span(parity, hid)]
+        return down_ref.at[span(parity * PARTS + kind - PARTS, down_part), :]
 
     def weight_place(kind, source):
-        if kind == 0:
-            return up_all.at[span(source, up_rows), :]
-        return down_all.at[source, (kind - 1) * part_rows : kind * part_rows, :]
+        if kind < PARTS:
+            return up_all.at[span(source * PARTS + kind, up_part), :]
+        return down_all.at[source, (kind - PARTS) * down_part : (kind - PARTS + 1) * down_part, :]
 
     def send_weight(kind, z_at, y_at, when=None):
         return sender.prepare(
             weight_src(kind, z_at), weight_place(kind, own), r_w.at[kind, own], dev(z_at=z_at, y_at=y_at), when
         )
 
-    down_kinds = tuple(range(1, 1 + DOWN_PARTS))
-
-    def below(kinds):
+    def below(kinds, last=1, first=z_count - 1):
         return [
             send_weight(kind, jnp.maximum(z - step, 0), y, z >= step)
+            for step in range(first, last - 1, -1)
             for kind in kinds
-            for step in range(z_count - 1, 0, -1)
         ]
 
     def above(kinds, step, odd=None):
@@ -648,14 +647,16 @@
         for start in starts:
             start()
 
-    issue(below((0,)))
-    for kind in (0, *down_kinds):
+    issue(below(up_kinds))
+    for kind in up_kinds + down_kinds:
         send_weight(kind, z, oy)()
     for part, ref in enumerate((wo_major, wo_minor)):
         sender.send(ref, wo_place(part, tp), r_wo.at[part, tp], dev(x_at=ox))
         sender.send(ref, wo_place(part, tp), r_wo.at[part, tp], dev(c_at=oc))
-    below_down = below(down_kinds)
-    near_up = above((0,), 1)
+    below_far, below_near = below(down_kinds, 2), below(down_kinds, 1, 1)
+    slow = (zl == 1) & (z > 1)
+    near_up = above(up_kinds, 1)
+    late_up = (zl == 0) & (z > 0)
 
     scales = (DK_MAJOR ** (-0.5) * LOG2_E, DK_MINOR ** (-0.5) * LOG2_E)
     lane = lax.broadcasted_iota(jnp.int32, (rows, width), 1)
@@ -731,10 +732,14 @@
             run_when(has_up, relay_copy(z_at, side, part).start)
 
     def after_last():
-        issue(near_up)
+        run_when(zl == 1, lambda: issue(near_up))
         for back in range(2, z_count):
             run_when(z >= back, lambda: credit(0, back))
-        issue(below_down)
+
+        @pl.when(jnp.logical_not(slow))
+        def _():
+            issue(below_far)
+            issue(below_near)
 
     for part in range(2):
         arrive(q_in.at[part], r_y.at[3 + part])
@@ -755,6 +760,7 @@
         z_at, key_side = z - 1 - index // 2, lax.rem(index, 2)
         pl.when(index > 1)(lambda: take(z_at, key_side))
         pl.when((index == 2 * z - 1) & (z > 1))(after_last)
+        pl.when((index == 2 * z - 2) & slow)(lambda: issue(below_far))
 
         def inner(side, carry):
             fold(side, z_at, key_side, False)
@@ -810,12 +816,11 @@
         sender.send(weight_place(kind, source), weight_place(kind, source), r_w.at[kind, source], dev(y_at=oy), when)
 
     for step in range(1, z_count):
-        pass_weight(0, lax.rem(z + step, z_count), z + step < z_count)
+        for kind in up_kinds:
+            pass_weight(kind, lax.rem(z + step, z_count), z + step < z_count)
     for step in range(2, z_count):
         run_when(z + step < z_count, lambda: await_credit(0, step))
-        issue(above((0,), step))
-    for step in range(2, z_count):
-        issue(above(down_kinds, step, 0))
+        issue(above(up_kinds, step))
 
     for made in local:
         made.wait()
@@ -864,16 +869,23 @@
     share(mine_at, z_peer)
     share(mine_at, x_peer)
     share(mine_at, partner)
+    run_when(late_up, lambda: issue(near_up))
+    run_when(slow, lambda: issue(below_near))
     issue(above(down_kinds, 1))
-    for step in range(1, z_count):
-        pass_weight(0, lax.rem(z + step, z_count), z + step >= z_count)
+    for step in range(1, z_count - 1):
+        for kind in up_kinds:
+            pass_weight(kind, lax.rem(z + step, z_count), z + step >= z_count)
     index = slot(c, ox, zl)
     arrive(rows_at(index), r_g.at[index])
     share(index, partner)
+    for step in range(2, z_count):
+        issue(above(down_kinds, step, 0))
     index = slot(c, x, 1 - zl)
     arrive(rows_at(index), r_g.at[index])
     share(index, x_peer)
     share(index, partner)
+    for kind in up_kinds:
+        pass_weight(kind, lax.rem(z + z_count - 1, z_count), z > 0)
     for back in range(2, z_count):
         run_when((z >= back) & (zl == 1), lambda: credit(1, back))
     index = slot(c, ox, 1 - zl)
@@ -881,7 +893,11 @@
     share(index, partner)
     for step in range(z_count):
         source = lax.rem(z + step, z_count) * y_count + oy
-        arrive(weight_place(0, source), r_w.at[0, source])
+        for kind in up_kinds:
+            arrive(weight_place(kind, source), r_w.at[kind, source])
+    for step in range(1, z_count):
+        for kind in down_kinds:
+            pass_weight(kind, lax.rem(z + step, z_count), z + step < z_count)
 
     for step in range(2, z_count):
         run_when((z + step < z_count) & (lax.rem(z + step, 2) == 1), lambda: await_credit(1, step))
@@ -908,6 +924,10 @@
             arrive(rows_at(index), r_g.at[index])
     expand(oc)
 
+    for step in range(1, z_count):
+        for kind in down_kinds:
+            pass_weight(kind, lax.rem(z + step, z_count), (z + step >= z_count) & jnp.logical_not(slow))
+
     x_rows = 2 * tile
     blocks = []
 
@@ -931,26 +951,23 @@
         out_ref[:, window] = total.astype(out_ref.dtype)
 
     def advance(t):
-        for stage, lag in ((stage_x, 1), (stage_z, 2), (stage_end, 3)):
+        for stage, lag in ((stage_x, 1), (stage_z, 4), (stage_end, 7)):
             if 0 <= t - lag < z_count * y_count:
                 stage(t - lag)
 
     def z_of(t):
-        return z - zl + 1 - t // 2 if t < 4 else lax.rem(z - zl + t // 2, z_count)
-
-    def pass_down(t):
+        return lax.rem(z - zl + 1 + t // 2, z_count)
+
+    late_pass = {}
+    for block in range(2, z_count * y_count, 2):
         for kind in down_kinds:
-            pass_weight(kind, z_of(t), z_of(t) != z if t < 4 else None)
-
-    early_pass = {0: (0, 2), 1: (4,)}
-    for t in range(2, z_count * y_count):
-        if 2 * t + 2 < z_count * y_count:
-            early_pass[t] = (2 * t + 2,)
+            at = block if kind > PARTS else max(block - 1, 0) if block > 2 else 0
+            late_pass.setdefault(at, []).append((block, kind))
     for t in range(z_count * y_count):
         source = z_of(t) * y_count + (oy if t % 2 else y)
         blocks.append(source)
-        for ahead in early_pass.get(t, ()):
-            pass_down(ahead)
+        for ahead, kind in late_pass.get(t, ()):
+            pass_weight(kind, z_of(ahead), slow)
         if t % 2:
             for kind in down_kinds:
                 arrive(weight_place(kind, source), r_w.at[kind, source])
@@ -960,7 +977,7 @@
         sender.send(d_send.at[t], d_in.at[t], r_d.at[t], partner)
         mine[t] = jnp.dot(hidden[span(c, group_rows), :], down_all[source], preferred_element_type=f32)
         advance(t)
-    for t in range(z_count * y_count, z_count * y_count + 3):
+    for t in range(z_count * y_count, z_count * y_count + 7):
         advance(t)
 
     sender.finish()
@@ -984,7 +1001,7 @@
     steps = sp_count
     bf16, f32 = jnp.bfloat16, jnp.float32
     dma = pltpu.SemaphoreType.DMA
-    sends = 160
+    sends = 192
     hbm = pl.BlockSpec(memory_space=pltpu.HBM)
     return pl.pallas_call(
         functools.partial(layer_kernel, (z_count, y_count, x_count)),
@@ -1022,7 +1039,7 @@
             dma((4,)),
             dma((5,)),
             dma((z_count, 2, 3)),
-            dma((1 + DOWN_PARTS, sp_count)),
+            dma((2 * PARTS, sp_count)),
             dma((2, tp_count)),
             dma((2, tp_count * y_count)),
             dma((2 * group_rows // tile,)),

time: 182 us -> 171 us (0.940)
  Pallas kernels: 179 us -> 168 us
    pallas_call x1, Pallas kernels: 179 us -> 168 us  [fused(): pl.pallas_call(functools.partial(layer_kernel, (z_count, y_count, x_count...]
where the time goes in v3:
time: 171 us
  Pallas kernels  168 us (98%)
  local copies, waits for them, and re-layouts  3.13 us (2%)
    pallas_call x1, Pallas kernels, fused(): pl.pallas_call(functools.partial(layer_kernel, (z_count, y_count, x_count...  168 us

profile of v3, /device:TPU:16, one launch (start us, length us, event | category | flops | bytes accessed | tf_op | source)
XLA Modules:
  0.0 170.8 jit_solution(12079261462760746080)
XLA Ops:
  0.0 0.0 copy-start
  0.0 0.7 copy-done
  0.7 0.6 broadcast_in_dim_tile.3.gain_minor
  1.3 167.7 %shard_map.154 = bf16[128,2048]{1,0:T(8,128)(2,1)} custom-call(bf16[128,2048]{1,0:T(8,128)(2,1)} %residual.1, bf16[512,256]{1,0:T(8,128)(2,1)} %q_major.1, bf16[512,256]{1,0:T(8,128)(2,1)} %k_major.1, bf16[512,256]{1,0:T(8,128)(2,1)} %v_major.1, bf16[512,128]{1,0:T(8,128)(2,1)} %q_minor.1, bf16[512,128]{1,0:T(8,128)(2,1)} %k_minor.1, ...), custom_call_target="tpu_custom_call" | custom-call | tf_op jit(solution)/shard_map/pallas_call | solution.py:1006
  168.9 1.9 %copy.18 = bf16[128,2048]{1,0:T(8,128)(2,1)} copy(bf16[128,2048]{1,0:T(8,128)(2,1)} %shard_map.154) | data formatting | bytes 1048576
  (1 shorter events, 0.0 us)
Async XLA Ops:
  0.0 0.7 copy-start

commit v4 on v3

--- a/solution.py
+++ b/solution.py
@@ -11,7 +11,9 @@
 DK_MINOR = 32
 SEGMENT = 64
 MAPS = 2
-PARTS = 2
+PART_UNITS = (4, 3, 2)
+PARTS = len(PART_UNITS)
+UNITS = 16
 
 EPSILON = 1e-06
 NEGATIVE = -1e30
@@ -534,7 +536,11 @@
     rows, tile = q_major.shape[0], residual.shape[0]
     width = q_minor.shape[1]
     half = width // 2
-    hid = up_ref.shape[1] // 2
+    unit = up_ref.shape[1] // UNITS
+    part_size = [units * unit for units in PART_UNITS]
+    part_at = [sum(part_size[:part]) for part in range(PARTS)]
+    big, small = sum(part_size), sum(part_size[:-1])
+    even = zl == 0
     up_rows = up_ref.shape[0]
     cols = down_ref.shape[1]
 
@@ -575,9 +581,26 @@
     kv_all[z, 1, span(y, rows), :] = v_major[:, span(y, width)]
     kv_all[z, 2, span(y, rows), :] = pack[y]
     local = []
+
+    def weight_src(kind, z_at):
+        part = kind % PARTS
+        start = pl.multiple_of(lax.rem(z_at, 2) * big + part_at[part], unit) if part < PARTS - 1 else part_at[part]
+        window = pl.ds(start, part_size[part])
+        return up_ref.at[:, window] if kind < PARTS else down_ref.at[window, :]
+
+    def weight_place(kind, source):
+        window = pl.ds(part_at[kind % PARTS], part_size[kind % PARTS])
+        return up_all.at[span(source, up_rows), window] if kind < PARTS else down_all.at[source, window, :]
+
+    def fits(kind, z_at, when):
+        if kind % PARTS < PARTS - 1:
+            return when
+        held = lax.rem(z_at, 2) == 0
+        return held if when is None else held & when
+
+    up_kinds, down_kinds = tuple(range(PARTS)), tuple(range(PARTS, 2 * PARTS))
     local_pairs = [
-        (up_ref.at[:, span(zl, hid)], up_all.at[span(own, up_rows), :]),
-        (down_ref.at[span(zl, hid), :], down_all.at[own]),
+        (weight_src(kind, z), weight_place(kind, own), fits(kind, z, None)) for kind in up_kinds + down_kinds
     ]
     major_rows, minor_rows = wo_major.shape[0], wo_minor.shape[0]
     tp_count = 2 * x_count
@@ -589,11 +612,11 @@
         return wo_all.at[pl.ds(pl.multiple_of(minor_base + index * minor_rows, minor_rows), minor_rows), :]
 
     for part, ref in enumerate((wo_major, wo_minor)):
-        local_pairs.append((ref, wo_place(part, tp)))
-    for slot, (src, dst) in enumerate(local_pairs):
-        made = pltpu.make_async_copy(src, dst, local_sem.at[slot])
-        made.start()
-        local.append(made)
+        local_pairs.append((ref, wo_place(part, tp), None))
+    for at, (src, dst, when) in enumerate(local_pairs):
+        made = pltpu.make_async_copy(src, dst, local_sem.at[at])
+        run_when(when, made.start)
+        local.append((when, made))
 
     pl.semaphore_wait(barrier, len(peers))
 
@@ -611,23 +634,13 @@
     for part, src in enumerate((k_major.at[:, span(y, width)], v_major.at[:, span(y, width)], pack.at[y])):
         sender.send(src, kv_place(z, part, y), r_kv.at[z, y, part], dev(z_at=next_z), has_up)
 
-    up_part, down_part = up_rows // PARTS, hid // PARTS
-    up_kinds, down_kinds = tuple(range(PARTS)), tuple(range(PARTS, 2 * PARTS))
-
-    def weight_src(kind, z_at):
-        parity = lax.rem(z_at, 2)
-        if kind < PARTS:
-            return up_ref.at[kind * up_part : (kind + 1) * up_part, span(parity, hid)]
-        return down_ref.at[span(parity * PARTS + kind - PARTS, down_part), :]
-
-    def weight_place(kind, source):
-        if kind < PARTS:
-            return up_all.at[span(source * PARTS + kind, up_part), :]
-        return down_all.at[source, (kind - PARTS) * down_part : (kind - PARTS + 1) * down_part, :]
-
     def send_weight(kind, z_at, y_at, when=None):
         return sender.prepare(
-            weight_src(kind, z_at), weight_place(kind, own), r_w.at[kind, own], dev(z_at=z_at, y_at=y_at), when
+            weight_src(kind, z_at),
+            weight_place(kind, own),
+            r_w.at[kind, own],
+            dev(z_at=z_at, y_at=y_at),
+            fits(kind, z_at, when),
         )
 
     def below(kinds, last=1, first=z_count - 1):
@@ -641,6 +654,8 @@
         when = z + step < z_count
         if odd is not None:
             when = when & (lax.rem(z + step, 2) == odd)
+        if odd == 1:
+            kinds = kinds[:-1]
         return [send_weight(kind, jnp.minimum(z + step, z_count - 1), y, when) for kind in kinds]
 
     def issue(starts):
@@ -653,7 +668,7 @@
     for part, ref in enumerate((wo_major, wo_minor)):
         sender.send(ref, wo_place(part, tp), r_wo.at[part, tp], dev(x_at=ox))
         sender.send(ref, wo_place(part, tp), r_wo.at[part, tp], dev(c_at=oc))
-    below_far, below_near = below(down_kinds, 2), below(down_kinds, 1, 1)
+    below_far, below_mid, below_near = below(down_kinds, 3), below(down_kinds, 2, 2), below(down_kinds, 1, 1)
     slow = (zl == 1) & (z > 1)
     near_up = above(up_kinds, 1)
     late_up = (zl == 0) & (z > 0)
@@ -738,8 +753,7 @@
 
         @pl.when(jnp.logical_not(slow))
         def _():
-            issue(below_far)
-            issue(below_near)
+            issue(below_far + below_mid + below_near)
 
     for part in range(2):
         arrive(q_in.at[part], r_y.at[3 + part])
@@ -760,6 +774,7 @@
         z_at, key_side = z - 1 - index // 2, lax.rem(index, 2)
         pl.when(index > 1)(lambda: take(z_at, key_side))
         pl.when((index == 2 * z - 1) & (z > 1))(after_last)
+        pl.when((index == 2 * z - 4) & slow)(lambda: issue(below_near))
         pl.when((index == 2 * z - 2) & slow)(lambda: issue(below_far))
 
         def inner(side, carry):
@@ -810,8 +825,12 @@
     cat[:, span(place, width)] = heads_out[0, token_span(y, x, c), :]
     minor_in[place] = heads_out[1, token_span(y, x, c), :]
 
+    def take_weight(kind, source):
+        run_when(fits(kind, z, None), lambda: arrive(weight_place(kind, source), r_w.at[kind, source]))
+
     def pass_weight(kind, z_at, when):
         source = z_at * y_count + y
+        when = fits(kind, z, when)
         run_when(when, lambda: arrive(weight_place(kind, source), r_w.at[kind, source]))
         sender.send(weight_place(kind, source), weight_place(kind, source), r_w.at[kind, source], dev(y_at=oy), when)
 
@@ -822,8 +841,8 @@
         run_when(z + step < z_count, lambda: await_credit(0, step))
         issue(above(up_kinds, step))
 
-    for made in local:
-        made.wait()
+    for when, made in local:
+        run_when(when, made.wait)
     for part in range(2):
         index = ox * 2 + c
         arrive(wo_place(part, index), r_wo.at[part, index])
@@ -870,11 +889,14 @@
     share(mine_at, x_peer)
     share(mine_at, partner)
     run_when(late_up, lambda: issue(near_up))
-    run_when(slow, lambda: issue(below_near))
+    run_when(slow, lambda: issue(below_mid))
     issue(above(down_kinds, 1))
     for step in range(1, z_count - 1):
         for kind in up_kinds:
             pass_weight(kind, lax.rem(z + step, z_count), z + step >= z_count)
+    for step in range(z_count - 1, 0, -1):
+        for kind in down_kinds:
+            pass_weight(kind, lax.rem(z + step, z_count), even & (z + step < z_count))
     index = slot(c, ox, zl)
     arrive(rows_at(index), r_g.at[index])
     share(index, partner)
@@ -888,20 +910,19 @@
         pass_weight(kind, lax.rem(z + z_count - 1, z_count), z > 0)
     for back in range(2, z_count):
         run_when((z >= back) & (zl == 1), lambda: credit(1, back))
+    for step in range(z_count - 1, 0, -1):
+        for kind in down_kinds[:-1]:
+            pass_weight(kind, lax.rem(z + step, z_count), (zl == 1) & ((z + step < z_count) | (z == 1)))
+    for step in range(2, z_count):
+        run_when((z + step < z_count) & (lax.rem(z + step, 2) == 1), lambda: await_credit(1, step))
+        issue(above(down_kinds, step, 1))
     index = slot(c, ox, 1 - zl)
     arrive(rows_at(index), r_g.at[index])
     share(index, partner)
     for step in range(z_count):
         source = lax.rem(z + step, z_count) * y_count + oy
         for kind in up_kinds:
-            arrive(weight_place(kind, source), r_w.at[kind, source])
-    for step in range(1, z_count):
-        for kind in down_kinds:
-            pass_weight(kind, lax.rem(z + step, z_count), z + step < z_count)
-
-    for step in range(2, z_count):
-        run_when((z + step < z_count) & (lax.rem(z + step, 2) == 1), lambda: await_credit(1, step))
-        issue(above(down_kinds, step, 1))
+            take_weight(kind, source)
 
     group_rows = 2 * x_count * tile
     hid_cols = 256
@@ -915,7 +936,16 @@
             hidden[span(side, group_rows), window] = jnp.square(jnp.maximum(pre, 0.0)).astype(bf16)
             return carry
 
-        lax.fori_loop(0, hid // hid_cols, one, 0)
+        full = jnp.where(even, big // hid_cols, small // hid_cols)
+        lax.fori_loop(0, full, one, 0)
+        rest = big % hid_cols
+        assert rest == small % hid_cols
+        if rest:
+            window = pl.ds(pl.multiple_of(full * hid_cols, hid_cols), rest)
+            pre = jnp.dot(
+                normed_all[span(side, group_rows), :], up_all[:, window], preferred_element_type=f32
+            )
+            hidden[span(side, group_rows), window] = jnp.square(jnp.maximum(pre, 0.0)).astype(bf16)
 
     expand(c)
     for x_at in range(x_count):
@@ -926,7 +956,7 @@
 
     for step in range(1, z_count):
         for kind in down_kinds:
-            pass_weight(kind, lax.rem(z + step, z_count), (z + step >= z_count) & jnp.logical_not(slow))
+            pass_weight(kind, lax.rem(z + step, z_count), even & (z + step >= z_count))
 
     x_rows = 2 * tile
     blocks = []
@@ -955,27 +985,38 @@
             if 0 <= t - lag < z_count * y_count:
                 stage(t - lag)
 
-    def z_of(t):
-        return lax.rem(z - zl + 1 + t // 2, z_count)
-
-    late_pass = {}
-    for block in range(2, z_count * y_count, 2):
-        for kind in down_kinds:
-            at = block if kind > PARTS else max(block - 1, 0) if block > 2 else 0
-            late_pass.setdefault(at, []).append((block, kind))
-    for t in range(z_count * y_count):
-        source = z_of(t) * y_count + (oy if t % 2 else y)
+    lower = [0, *range(z_count - 1, 0, -1)]
+    upper = [*range(1, z_count - 1), 0, z_count - 1]
+
+    def z_of(block):
+        return lax.rem(z - zl + jnp.where(z < 2, lower[block], upper[block]), z_count)
+
+    count = z_count
+    order = [(0, 0), (0, 1), (1, 0)]
+    for block in range(2, count):
+        order += [(block, 0), (block - 1, 1)]
+    order.append((count - 1, 1))
+    for t, (block, side) in enumerate(order):
+        source = z_of(block) * y_count + (oy if side else y)
         blocks.append(source)
-        for ahead, kind in late_pass.get(t, ()):
+        for ahead, kind in ([(1, PARTS)] if t == 0 else []) + [
+            (block, kind) for kind in down_kinds[:-1] if block and not side and (block > 1 or kind > PARTS)
+        ]:
             pass_weight(kind, z_of(ahead), slow)
-        if t % 2:
+        if side:
             for kind in down_kinds:
-                arrive(weight_place(kind, source), r_w.at[kind, source])
-        d_send[t] = jnp.dot(
-            hidden[span(oc, group_rows), :], down_all[source], preferred_element_type=f32
-        ).astype(bf16)
-        sender.send(d_send.at[t], d_in.at[t], r_d.at[t], partner)
-        mine[t] = jnp.dot(hidden[span(c, group_rows), :], down_all[source], preferred_element_type=f32)
+                take_weight(kind, source)
+        start = sender.prepare(d_send.at[t], d_in.at[t], r_d.at[t], partner)
+
+        def multiply(depth):
+            block = down_all[source, :depth, :]
+            sent = jnp.dot(hidden[span(oc, group_rows), :depth], block, preferred_element_type=f32)
+            d_send[t] = sent.astype(bf16)
+            start()
+            mine[t] = jnp.dot(hidden[span(c, group_rows), :depth], block, preferred_element_type=f32)
+
+        pl.when(even)(lambda: multiply(big))
+        pl.when(jnp.logical_not(even))(lambda: multiply(small))
         advance(t)
     for t in range(z_count * y_count, z_count * y_count + 7):
         advance(t)
@@ -994,7 +1035,8 @@
     z_count, y_count = grid_sizes(sp_count)
     x_count = tp_count // 2
     rows, tile, width = q_major.shape[0], residual.shape[0], q_minor.shape[1]
-    model, hid = residual.shape[1], up_weight.shape[1] // 2
+    model = residual.shape[1]
+    hid = up_weight.shape[1] // UNITS * sum(PART_UNITS)
     cols = down_weight.shape[1]
     features = tp_count * (wo_major.shape[0] + wo_minor.shape[0])
     group_rows = 2 * x_count * tile
@@ -1036,7 +1078,7 @@
             pltpu.VMEM((steps, tile, cols), f32),
             dma((sends,)),
             dma((z_count, 2, 3)),
-            dma((4,)),
+            dma((2 * PARTS + 2,)),
             dma((5,)),
             dma((z_count, 2, 3)),
             dma((2 * PARTS, sp_count)),
@@ -1065,6 +1107,7 @@
         and width == 2 * MAPS * DK_MINOR
         and width == MAPS * DK_MAJOR
         and width % 128 == 0
+        and args[14].shape[1] % (UNITS * 128) == 0
         and v_minor.shape[1] == width
         and q_major.shape[1] == v_major.shape[1] == 2 * width
     )

time: 171 us -> 159 us (0.930)
  Pallas kernels: 168 us -> 156 us
    pallas_call x1, Pallas kernels: 168 us -> 156 us  [fused(): pl.pallas_call(functools.partial(layer_kernel, (z_count, y_count, x_count...]
where the time goes in v4:
time: 159 us
  Pallas kernels  156 us (98%)
  local copies, waits for them, and re-layouts  3.13 us (2%)
    pallas_call x1, Pallas kernels, fused(): pl.pallas_call(functools.partial(layer_kernel, (z_count, y_count, x_count...  156 us

profile of v4, /device:TPU:16, one launch (start us, length us, event | category | flops | bytes accessed | tf_op | source)
XLA Modules:
  0.0 158.9 jit_solution(12376753216594882764)
XLA Ops:
  0.0 0.0 copy-start
  0.0 0.7 copy-done
  0.7 0.6 broadcast_in_dim_tile.3.gain_minor
  1.3 155.8 %shard_map.154 = bf16[128,2048]{1,0:T(8,128)(2,1)} custom-call(bf16[128,2048]{1,0:T(8,128)(2,1)} %residual.1, bf16[512,256]{1,0:T(8,128)(2,1)} %q_major.1, bf16[512,256]{1,0:T(8,128)(2,1)} %k_major.1, bf16[512,256]{1,0:T(8,128)(2,1)} %v_major.1, bf16[512,128]{1,0:T(8,128)(2,1)} %q_minor.1, bf16[512,128]{1,0:T(8,128)(2,1)} %k_minor.1, ...), custom_call_target="tpu_custom_call" | custom-call | tf_op jit(solution)/shard_map/pallas_call | solution.py:1048
  157.1 1.9 %copy.18 = bf16[128,2048]{1,0:T(8,128)(2,1)} copy(bf16[128,2048]{1,0:T(8,128)(2,1)} %shard_map.154) | data formatting | bytes 1048576
  (1 shorter events, 0.0 us)
Async XLA Ops:
  0.0 0.7 copy-start

commit v5 on v4

--- a/solution.py
+++ b/solution.py
@@ -560,12 +560,6 @@
             device_id_type=pl.DeviceIdType.MESH,
         ).wait_recv()
 
-    k_low = lax.broadcasted_iota(jnp.int32, (rows, width), 1)
-    for head in range(2):
-        k_part = (k_low >= head * half) & (k_low < (head + 1) * half)
-        turned_v = pltpu.roll(v_minor[...].astype(f32), half, 1)
-        pack[head] = jnp.where(k_part, k_minor[...].astype(f32), turned_v).astype(bf16)
-
     barrier = pltpu.get_barrier_semaphore()
     peers = []
     for dy in range(2):
@@ -576,6 +570,12 @@
     peers += [dev(z_at=lax.rem(z + step, z_count)) for step in range(1, z_count)]
     for peer in peers:
         pl.semaphore_signal(barrier, inc=1, device_id=peer, device_id_type=pl.DeviceIdType.MESH)
+
+    k_low = lax.broadcasted_iota(jnp.int32, (rows, width), 1)
+    for head in range(2):
+        k_part = (k_low >= head * half) & (k_low < (head + 1) * half)
+        turned_v = pltpu.roll(v_minor[...].astype(f32), half, 1)
+        pack[head] = jnp.where(k_part, k_minor[...].astype(f32), turned_v).astype(bf16)
 
     kv_all[z, 0, span(y, rows), :] = k_major[:, span(y, width)]
     kv_all[z, 1, span(y, rows), :] = v_major[:, span(y, width)]
@@ -788,7 +788,7 @@
 
     value_row = lax.broadcasted_iota(jnp.int32, (width, rows), 0)
     value_keep = (value_row >= oy * half) & (value_row < (oy + 1) * half)
-    gains = (gain_major[...], gain_minor[...])
+    gains = (gain_major[...], jnp.concatenate([gain_minor[...], gain_minor[...]], axis=1))
     lams = (lam_major[y], lam_minor[y])
 
     def close(side, carry):
@@ -980,10 +980,13 @@
         total = stream[:, window] + (z_keep[t] + z_in[blocks[t]].astype(f32))
         out_ref[:, window] = total.astype(out_ref.dtype)
 
-    def advance(t):
-        for stage, lag in ((stage_x, 1), (stage_z, 4), (stage_end, 7)):
-            if 0 <= t - lag < z_count * y_count:
-                stage(t - lag)
+    reached = {stage_x: 0, stage_z: 0, stage_end: 0}
+
+    def advance(*targets):
+        for stage, target in zip((stage_x, stage_z, stage_end), targets):
+            while reached[stage] < min(target, z_count * y_count):
+                stage(reached[stage])
+                reached[stage] += 1
 
     lower = [0, *range(z_count - 1, 0, -1)]
     upper = [*range(1, z_count - 1), 0, z_count - 1]
@@ -996,13 +999,18 @@
     for block in range(2, count):
         order += [(block, 0), (block - 1, 1)]
     order.append((count - 1, 1))
+    late_pass = {0: [(count - 2, PARTS)], 1: [(1, PARTS)], 2: [(1, kind) for kind in down_kinds[1:-1]]}
+    for t, (block, side) in enumerate(order):
+        if block > 1 and not side:
+            first = PARTS + 1 if block == count - 2 else PARTS
+            late_pass[t] = [(block, kind) for kind in range(first, 2 * PARTS - 1)]
     for t, (block, side) in enumerate(order):
         source = z_of(block) * y_count + (oy if side else y)
         blocks.append(source)
-        for ahead, kind in ([(1, PARTS)] if t == 0 else []) + [
-            (block, kind) for kind in down_kinds[:-1] if block and not side and (block > 1 or kind > PARTS)
-        ]:
+        for ahead, kind in late_pass.get(t, ()):
             pass_weight(kind, z_of(ahead), slow)
+        if t == len(order) - 1:
+            advance(t, t - 2, t - 6)
         if side:
             for kind in down_kinds:
                 take_weight(kind, source)
@@ -1017,9 +1025,10 @@
 
         pl.when(even)(lambda: multiply(big))
         pl.when(jnp.logical_not(even))(lambda: multiply(small))
-        advance(t)
-    for t in range(z_count * y_count, z_count * y_count + 7):
-        advance(t)
+        advance(t, t - 3, t - 6)
+    for t in range(len(order) + 1):
+        advance(len(order), t, t - 1)
+    advance(len(order), len(order), len(order))
 
     sender.finish()
     for step in range(1, z_count):
@@ -1107,6 +1116,7 @@
         and width == 2 * MAPS * DK_MINOR
         and width == MAPS * DK_MAJOR
         and width % 128 == 0
+        and z_count >= 4
         and args[14].shape[1] % (UNITS * 128) == 0
         and v_minor.shape[1] == width
         and q_major.shape[1] == v_major.shape[1] == 2 * width
@@ -1143,7 +1153,7 @@
         lambda_major,
         lambda_minor,
         gain_major[None, :],
-        jnp.tile(gain_minor, 2)[None, :],
+        gain_minor[None, :],
         output_major,
         output_minor,
         mixer_gain[None, :],

time: 159 us -> 157 us (0.987)
  no operation moved by 1% of the time
where the time goes in v5:
time: 157 us
  Pallas kernels  155 us (99%)
  local copies, waits for them, and re-layouts  1.88 us (1%)
    pallas_call x1, Pallas kernels, fused(): pl.pallas_call(functools.partial(layer_kernel, (z_count, y_count, x_count...  155 us

profile of v5, /device:TPU:16, one launch (start us, length us, event | category | flops | bytes accessed | tf_op | source)
XLA Modules:
  0.0 156.7 jit_solution(12431518036960526095)
XLA Ops:
  0.0 154.8 %shard_map.154 = bf16[128,2048]{1,0:T(8,128)(2,1)} custom-call(bf16[128,2048]{1,0:T(8,128)(2,1)} %residual.1, bf16[512,256]{1,0:T(8,128)(2,1)} %q_major.1, bf16[512,256]{1,0:T(8,128)(2,1)} %k_major.1, bf16[512,256]{1,0:T(8,128)(2,1)} %v_major.1, bf16[512,128]{1,0:T(8,128)(2,1)} %q_minor.1, bf16[512,128]{1,0:T(8,128)(2,1)} %k_minor.1, ...), custom_call_target="tpu_custom_call" | custom-call | tf_op jit(solution)/shard_map/pallas_call | solution.py:1057
  154.8 1.9 %copy.18 = bf16[128,2048]{1,0:T(8,128)(2,1)} copy(bf16[128,2048]{1,0:T(8,128)(2,1)} %shard_map.154) | data formatting | bytes 1048576

commit v6 on v5

--- a/solution.py
+++ b/solution.py
@@ -11,7 +11,7 @@
 DK_MINOR = 32
 SEGMENT = 64
 MAPS = 2
-PART_UNITS = (4, 3, 2)
+PART_UNITS = (3, 3, 4)
 PARTS = len(PART_UNITS)
 UNITS = 16
 

time: 157 us -> 162 us (1.032)
  Pallas kernels: 155 us -> 160 us
    pallas_call x1, Pallas kernels: 155 us -> 160 us  [fused(): pl.pallas_call(functools.partial(layer_kernel, (z_count, y_count, x_count...]
where the time goes in v6:
time: 162 us
  Pallas kernels  160 us (99%)
  local copies, waits for them, and re-layouts  1.88 us (1%)
    pallas_call x1, Pallas kernels, fused(): pl.pallas_call(functools.partial(layer_kernel, (z_count, y_count, x_count...  160 us

profile of v6, /device:TPU:16, one launch (start us, length us, event | category | flops | bytes accessed | tf_op | source)
XLA Modules:
  0.0 162.0 jit_solution(4857184616441421610)
XLA Ops:
  0.0 160.1 %shard_map.154 = bf16[128,2048]{1,0:T(8,128)(2,1)} custom-call(bf16[128,2048]{1,0:T(8,128)(2,1)} %residual.1, bf16[512,256]{1,0:T(8,128)(2,1)} %q_major.1, bf16[512,256]{1,0:T(8,128)(2,1)} %k_major.1, bf16[512,256]{1,0:T(8,128)(2,1)} %v_major.1, bf16[512,128]{1,0:T(8,128)(2,1)} %q_minor.1, bf16[512,128]{1,0:T(8,128)(2,1)} %k_minor.1, ...), custom_call_target="tpu_custom_call" | custom-call | tf_op jit(solution)/shard_map/pallas_call | solution.py:1057
  160.1 1.9 %copy.18 = bf16[128,2048]{1,0:T(8,128)(2,1)} copy(bf16[128,2048]{1,0:T(8,128)(2,1)} %shard_map.154) | data formatting | bytes 1048576
